TPU v7x, 32 devices: a whole 2x2x4 slice. The times are simulated.
32 devices in a mesh: sp: 8 (over z, x), tp: 4 (over y, core).
Axes of the slice: x: 2, y: 2, z: 4, core: 2. Of those that a mesh axis runs over, the one named last changes fastest.
Arguments:
- queries: bfloat16 [8192, 2048], P('sp', 'tp'), may hold values from -16 to 16
- key_rows: bfloat16 [8192, 512], P('sp', 'tp'), may hold values from -16 to 16
- value_rows: bfloat16 [8192, 512], P('sp', 'tp'), may hold values from -6 to 6
- doc_ids: int32 [8192], P('sp'), may hold values from 0 to 3, never falling along the last dimension, each value on 1 to 4096 neighbouring positions
- sink_logit: float32 [32], P('tp'), may hold values from 3 to 7
- residual: bfloat16 [8192, 2048], P(('sp', 'tp')), may hold values from -6 to 6
- out_weight: bfloat16 [2048, 2048], P('tp'), may hold values from -3.5 to 3.5
- norm_gain: float32 [2048], replicated, may hold values from 0.1 to 1.9
- gate_weight: bfloat16 [8, 2048, 512], P('sp'), may hold values from -0.125 to 0.125
- up_weight: bfloat16 [8, 2048, 512], P('sp'), may hold values from -0.125 to 0.125
- down_weight: bfloat16 [8, 512, 2048], P('sp'), may hold values from -0.25 to 0.25
- routes: int32 [8192, 2], P(('sp', 'tp')), may hold values from 0 to 7, as said below
- route_weights: float32 [8192, 2], P(('sp', 'tp')), may hold values from 0.2 to 0.8
Outputs:
- mixed: bfloat16 [8192, 2048], P(('sp', 'tp'))
Inputs may be any that keep to these rules, and one draw needn't show every extreme that they name: `doc_ids`: never falls along the positions. `routes`: each aligned block of 256 rows names every expert exactly 64 times; the experts of one row differ and lie in one group of 2 consecutive numbers.
All inputs are finite; a program needn't handle non-finite values.
Results may differ from a plain program's by a relative error of at most 0.012.
Values may be sent and summed in bfloat16 or wider, within the bound.
A program may use at most 128 MiB of HBM per device.

v0:
```python
import functools

import jax
import jax.numpy as jnp
from jax import lax
from jax.experimental import pallas as pl
from jax.experimental.pallas import tpu as pltpu
from jax.sharding import PartitionSpec as P

HD = 64
WINDOW = 128
GROUPS = 4
CHUNKS = 4


neg_fill = -1e30
eps_norm = 1e-06


def extended(block, sides, width):
    for axis, dim in sides:
        count = lax.axis_size(axis)
        forward = [(i, i + 1) for i in range(count - 1)]
        backward = [(target, source) for source, target in forward]
        low = lax.ppermute(
            lax.slice_in_dim(block, block.shape[dim] - width, None, axis=dim), axis, forward
        )
        high = lax.ppermute(lax.slice_in_dim(block, 0, width, axis=dim), axis, backward)
        block = jnp.concatenate([low, block, high], axis=dim)
    return block


def attend(
    query_part,
    key_part,
    value_part,
    query_docs,
    key_docs,
    query_start,
    key_start,
    sink_logit,
    extent,
):
    query_count = query_part.shape[0]
    key_count = key_part.shape[0]
    groups = key_part.shape[1] // HD
    head_ratio = sink_logit.shape[0] // groups
    query_heads = query_part.reshape(query_count, groups, head_ratio, HD)
    key_heads = key_part.reshape(key_count, groups, HD)
    value_heads = value_part.reshape(key_count, groups, HD)
    scores = jnp.einsum(
        "qgrd,kgd->grqk", query_heads, key_heads, preferred_element_type=jnp.float32
    ) * HD ** (-0.5)
    query_pos = query_start + jnp.arange(query_count, dtype=jnp.int32)
    key_pos = key_start + jnp.arange(key_count, dtype=jnp.int32)
    inside = (key_pos >= 0) & (key_pos < extent)
    allowed = (
        (jnp.abs(query_pos[:, None] - key_pos[None, :]) <= WINDOW)
        & (query_docs[:, None] == key_docs[None, :])
        & inside[None, :]
    )
    masked = jnp.where(allowed[None, None], scores, neg_fill)
    sink_col = sink_logit.reshape(groups, head_ratio)[:, :, None, None]
    row_top = jnp.maximum(jnp.max(masked, axis=3, keepdims=True), sink_col)
    exponent = jnp.where(allowed[None, None], jnp.exp(masked - row_top), 0.0)
    denominator = jnp.sum(exponent, axis=3, keepdims=True) + jnp.exp(sink_col - row_top)
    attn_weight = (exponent / denominator).astype(jnp.bfloat16)
    attended = jnp.einsum(
        "grqk,kgd->qgrd", attn_weight, value_heads, preferred_element_type=jnp.float32
    )
    return attended.astype(jnp.bfloat16).reshape(query_count, -1)


def fetch_margins(key_rows, value_rows, doc_float):
    return (
        extended(key_rows, (("sp", 0),), WINDOW),
        extended(value_rows, (("sp", 0),), WINDOW),
        extended(doc_float, (("sp", 0),), WINDOW),
    )


def moe_kernel(
    groups, chunks,
    sink_ref, q_ref, k_ref, v_ref, doc_ref, res_ref, w_ref,
    gain_ref, routes_ref, rw_ref, gate_hbm, up_hbm, down_hbm,
    out_ref,
    kx, vx, dl, dr, dx, att, am_far, am_near, w_mate, acc, ysend, yrecv,
    hs, hr, ms, mr, ys, yr,
    stream_ref, send, own, peer, pout, pin, comb, ret, wsend, wown, wpeer,
    gv, uv, dv, acc_g, acc_u,
    zs, zr, xs, xr, zws, zwr, xws, xwr, bzs, bzr, bxs, bxr, wsem,
):
    me = lax.axis_index("sp")
    gz = me // 2
    side = me % 2
    mate = gz * 2 + 1 - side
    rows, width = res_ref.shape
    cap = rows // groups
    cw = width // chunks
    half = groups // 2
    offsets = [half] + [d for d in range(groups - 1, 0, -1) if d != half]

    def remote(src, dst, ss, rs, target):
        return pltpu.make_async_remote_copy(
            src_ref=src, dst_ref=dst, send_sem=ss, recv_sem=rs,
            device_id={"sp": target}, device_id_type=pl.DeviceIdType.MESH,
        )

    barrier = pltpu.get_barrier_semaphore()
    for d in offsets:
        pl.semaphore_signal(
            barrier, inc=1, device_id={"sp": ((gz + d) % groups) * 2 + side},
            device_id_type=pl.DeviceIdType.MESH,
        )
    pl.semaphore_signal(
        barrier, inc=1, device_id={"sp": mate}, device_id_type=pl.DeviceIdType.MESH
    )
    loads = [
        pltpu.make_async_copy(s.at[0], t, wsem.at[i])
        for i, (s, t) in enumerate(((gate_hbm, gv), (up_hbm, uv), (down_hbm, dv)))
    ]
    for load in loads:
        load.start()

    first = routes_ref[:, 0:1]
    group_of = first // 2
    lanes = lax.broadcasted_iota(jnp.int32, (rows, 128), 1)
    one_hot = jnp.where(group_of == lanes, 1.0, 0.0)
    ri = lax.broadcasted_iota(jnp.int32, (rows, rows), 0)
    ci = lax.broadcasted_iota(jnp.int32, (rows, rows), 1)
    below = jnp.where(ci < ri, 1.0, 0.0).astype(jnp.bfloat16)
    ranks = jnp.dot(below, one_hot.astype(jnp.bfloat16), preferred_element_type=jnp.float32)
    slot = group_of.astype(jnp.float32) * cap + jnp.sum(ranks * one_hot, axis=1, keepdims=True)
    spread = jnp.where(slot == ci.astype(jnp.float32), 1.0, 0.0)
    spread_b = spread.astype(jnp.bfloat16)
    slot_lane = jnp.sum(jnp.where(ri == ci, slot, 0.0), axis=0, keepdims=True)
    pick = jnp.where(ri.astype(jnp.float32) == slot_lane, 1.0, 0.0).astype(jnp.bfloat16)
    for parity in range(2):
        w_col = jnp.where(first % 2 == parity, rw_ref[:, 0:1], rw_ref[:, 1:2])
        w_row = jnp.sum(spread * w_col, axis=0, keepdims=True)
        wsend[parity] = jnp.broadcast_to(w_row, (8, rows))

    pending = []

    def entered():
        for d in offsets:
            copy = remote(
                wsend, wown.at[gz], zws.at[d], zwr.at[gz], ((gz + d) % groups) * 2 + side
            )
            copy.start()
            pending.append(copy)
        copy = remote(wsend, wpeer.at[gz], xws.at[gz], xwr.at[gz], mate)
        copy.start()
        pending.append(copy)

    def emit(j):
        rows_j = stream_ref[:, j * cw:(j + 1) * cw]
        piece = jnp.dot(pick, rows_j, preferred_element_type=jnp.float32)
        send[j] = piece.astype(jnp.bfloat16).reshape(groups, cap, cw)
        for d in offsets:
            target = (gz + d) % groups
            copy = remote(
                send.at[j, target], own.at[j, gz], zs.at[j, d], zr.at[j, gz], target * 2 + side
            )
            copy.start()
            pending.append(copy)
        copy = remote(send.at[j, gz], peer.at[j, gz], xs.at[j, gz], xr.at[j, gz], mate)
        copy.start()
        pending.append(copy)
        own[j, pl.ds(gz, 1)] = send[j, pl.ds(gz, 1)]

    front_kernel(
        chunks, groups, entered, emit,
        sink_ref, q_ref, k_ref, v_ref, doc_ref, res_ref, w_ref,
        stream_ref,
        kx, vx, dl, dr, dx, att, am_far, am_near, w_mate, acc, ysend, yrecv,
        hs, hr, ms, mr, ys, yr,
    )
    wown[pl.ds(gz, 1)] = wsend[...][None]

    for d in offsets:
        source = (gz + groups - d) % groups
        remote(wsend, wown.at[source], zws.at[d], zwr.at[source], mate).wait_recv()
        copy = remote(wown.at[source], wpeer.at[source], xws.at[source], xwr.at[source], mate)
        copy.start()
        pending.append(copy)

    loads[0].wait()
    loads[1].wait()

    squares = {0: 0.0, rows: 0.0}

    def accumulate(buf, j, base):
        wide = buf[j].reshape(rows, cw).astype(jnp.float32)
        squares[base] = squares[base] + jnp.sum(wide * wide, axis=1, keepdims=True)
        block = (wide * gain_ref[:, j * cw:(j + 1) * cw]).astype(jnp.bfloat16)
        part_g = jnp.dot(block, gv[j * cw:(j + 1) * cw, :], preferred_element_type=jnp.float32)
        part_u = jnp.dot(block, uv[j * cw:(j + 1) * cw, :], preferred_element_type=jnp.float32)
        if j == 0:
            acc_g[base:base + rows, :] = part_g
            acc_u[base:base + rows, :] = part_u
        else:
            acc_g[base:base + rows, :] += part_g
            acc_u[base:base + rows, :] += part_u

    def peer_step(j):
        for s in range(groups):
            remote(send.at[j, s], peer.at[j, s], xs.at[j, s], xr.at[j, s], mate).wait_recv()
        accumulate(peer, j, rows)

    for j in range(chunks):
        for d in offsets:
            source = (gz + groups - d) % groups
            remote(
                send.at[j, source], own.at[j, source], zs.at[j, d], zr.at[j, source], mate
            ).wait_recv()
            copy = remote(
                own.at[j, source], peer.at[j, source], xs.at[j, source], xr.at[j, source], mate
            )
            copy.start()
            pending.append(copy)
        accumulate(own, j, 0)
        if j:
            peer_step(j - 1)
    peer_step(chunks - 1)
    for s in range(groups):
        remote(wsend, wpeer.at[s], xws.at[s], xwr.at[s], mate).wait_recv()

    def hidden_of(base):
        scale = lax.rsqrt(squares[base] / width + eps_norm)
        g = acc_g[base:base + rows, :] * scale
        u = acc_u[base:base + rows, :] * scale
        return (g / (1.0 + jnp.exp(-g)) * u).astype(jnp.bfloat16)

    sub = lax.broadcasted_iota(jnp.int32, (cap, rows), 0)
    lane = lax.broadcasted_iota(jnp.int32, (cap, rows), 1)
    chosen = lane == sub + gz * cap

    def weights_of(buf):
        cols = []
        for s in range(groups):
            row = jnp.where(side == 0, buf[s, 0, 0:1, :], buf[s, 1, 0:1, :])
            cols.append(jnp.sum(jnp.where(chosen, row, 0.0), axis=1, keepdims=True))
        return jnp.concatenate(cols, axis=0)

    w_peer = weights_of(wpeer)
    hid_peer = hidden_of(rows)
    loads[2].wait()
    for j in range(chunks):
        part = jnp.dot(hid_peer, dv[:, j * cw:(j + 1) * cw], preferred_element_type=jnp.float32)
        pout[j] = (part * w_peer).astype(jnp.bfloat16)
        copy = remote(pout.at[j], pin.at[j], bxs.at[j], bxr.at[j], mate)
        copy.start()
        pending.append(copy)
    w_own = weights_of(wown)
    hid_own = hidden_of(0)
    for j in range(chunks):
        part = jnp.dot(hid_own, dv[:, j * cw:(j + 1) * cw], preferred_element_type=jnp.float32)
        remote(pout.at[j], pin.at[j], bxs.at[j], bxr.at[j], mate).wait_recv()
        total = part * w_own + pin[j].astype(jnp.float32)
        comb[j] = total.astype(jnp.bfloat16).reshape(groups, cap, cw)
        for d in offsets:
            target = (gz + d) % groups
            copy = remote(
                comb.at[j, target], ret.at[j, gz], bzs.at[j, d], bzr.at[j, gz], target * 2 + side
            )
            copy.start()
            pending.append(copy)
        ret[j, pl.ds(gz, 1)] = comb[j, pl.ds(gz, 1)]
    for j in range(chunks):
        for d in offsets:
            source = (gz + groups - d) % groups
            remote(
                comb.at[j, source], ret.at[j, source], bzs.at[j, d], bzr.at[j, source], mate
            ).wait_recv()
        back = jnp.dot(spread_b, ret[j].reshape(rows, cw), preferred_element_type=jnp.float32)
        cols = slice(j * cw, (j + 1) * cw)
        out_ref[:, cols] = (stream_ref[:, cols].astype(jnp.float32) + back).astype(jnp.bfloat16)
    for copy in pending:
        copy.wait_send()


def front_kernel(
    chunks, extra, entered, emit,
    sink_ref, q_ref, k_ref, v_ref, doc_ref, res_ref, w_ref,
    out_ref,
    kx, vx, dl, dr, dx, att, am_far, am_near, w_mate, acc, ysend, yrecv,
    hs, hr, ms, mr, ys, yr,
):
    sp = lax.axis_index("sp")
    tp = lax.axis_index("tp")
    sp_count = lax.axis_size("sp")
    mate = tp + 1 - 2 * (tp % 2)
    across = (tp + 2) % 4
    mate_across = (mate + 2) % 4
    after = (sp + 1) % sp_count
    before = (sp + sp_count - 1) % sp_count
    blocks = q_ref.shape[0] // WINDOW
    home_blocks = blocks // 4
    half = blocks // 2
    kv_heads = k_ref.shape[1] // HD
    ratio = q_ref.shape[1] // k_ref.shape[1]
    width = out_ref.shape[1]
    cw = width // chunks
    f32, bf = jnp.float32, jnp.bfloat16
    mesh_id = pl.DeviceIdType.MESH

    def remote(src, dst, ss, rs, where):
        return pltpu.make_async_remote_copy(
            src_ref=src, dst_ref=dst, send_sem=ss, recv_sem=rs,
            device_id=where, device_id_type=mesh_id,
        )

    barrier = pltpu.get_barrier_semaphore()
    for where in ({"sp": after}, {"sp": before}, {"tp": mate}, {"tp": across}):
        pl.semaphore_signal(barrier, inc=1, device_id=where, device_id_type=mesh_id)
    for b in range(blocks):
        kx[b + 1] = k_ref[b * WINDOW:(b + 1) * WINDOW, :]
        vx[b + 1] = v_ref[b * WINDOW:(b + 1) * WINDOW, :]
        dx[b + 1] = jnp.broadcast_to(doc_ref[b:b + 1, :].astype(f32), (8, WINDOW))
    pl.semaphore_wait(barrier, 4 + extra)

    tail = pl.ds((blocks - 1) * WINDOW, WINDOW)
    lead = pl.ds(0, WINDOW)
    halo = [
        remote(k_ref.at[tail], kx.at[0], hs.at[0], hr.at[0], {"sp": after}),
        remote(v_ref.at[tail], vx.at[0], hs.at[1], hr.at[1], {"sp": after}),
        remote(doc_ref, dl, hs.at[2], hr.at[2], {"sp": after}),
        remote(k_ref.at[lead], kx.at[blocks + 1], hs.at[3], hr.at[3], {"sp": before}),
        remote(v_ref.at[lead], vx.at[blocks + 1], hs.at[4], hr.at[4], {"sp": before}),
        remote(doc_ref, dr, hs.at[5], hr.at[5], {"sp": before}),
    ]
    for copy in halo:
        copy.start()
    w_copy = remote(w_ref, w_mate, ms.at[0], mr.at[0], {"tp": mate})
    w_copy.start()
    if entered is not None:
        entered()

    qi = lax.broadcasted_iota(jnp.int32, (WINDOW, 3 * WINDOW), 0)
    ki = lax.broadcasted_iota(jnp.int32, (WINDOW, 3 * WINDOW), 1)
    band = (ki >= qi) & (ki <= qi + 2 * WINDOW)
    eye = lax.broadcasted_iota(jnp.int32, (WINDOW, WINDOW), 0) == lax.broadcasted_iota(
        jnp.int32, (WINDOW, WINDOW), 1
    )

    def attend_block(b):
        own_docs = dx[b + 1][0:1]
        key_docs = jnp.concatenate([dx[b][0:1], own_docs, dx[b + 2][0:1]], axis=1)
        query_docs = jnp.sum(jnp.where(eye, own_docs, 0.0), axis=1, keepdims=True)
        bias = jnp.where(band & (key_docs == query_docs), 0.0, neg_fill)
        keys = kx[pl.ds(b, 3)].reshape(3 * WINDOW, kv_heads * HD)
        values = vx[pl.ds(b, 3)].reshape(3 * WINDOW, kv_heads * HD)
        home = b // home_blocks
        to_rows = pl.ds(pl.multiple_of((b % home_blocks) * WINDOW, WINDOW), WINDOW)
        from_rows = pl.ds(pl.multiple_of(b * WINDOW, WINDOW), WINDOW)
        for g in range(kv_heads):
            span = slice(g * ratio * HD, (g + 1) * ratio * HD)
            q = q_ref[from_rows, span] * jnp.asarray(HD ** (-0.5), bf)
            stacked = jnp.concatenate([q[:, r * HD:(r + 1) * HD] for r in range(ratio)], axis=0)
            scores = lax.dot_general(
                stacked, keys[:, g * HD:(g + 1) * HD], (((1,), (1,)), ((), ())),
                preferred_element_type=f32,
            )
            vg = values[:, g * HD:(g + 1) * HD]
            parts = []
            for r in range(ratio):
                sink = sink_ref[g * ratio + r]
                s = scores[r * WINDOW:(r + 1) * WINDOW] + bias
                top = jnp.maximum(jnp.max(s, axis=1, keepdims=True), sink)
                e = jnp.exp(s - top)
                den = jnp.sum(e, axis=1, keepdims=True) + jnp.exp(sink - top)
                o = jnp.dot(e.astype(bf), vg, preferred_element_type=f32)
                parts.append((o / den).astype(bf))
            att[home, to_rows, span] = jnp.concatenate(parts, axis=1)

    def far_step(i, carry):
        @pl.when(i == half - 1)
        def _():
            for copy in halo:
                copy.wait_recv()
            left = dl[blocks - 1:blocks, :].astype(f32)
            right = dr[0:1, :].astype(f32)
            left = jnp.where(sp == 0, -1.0, left)
            right = jnp.where(sp == sp_count - 1, -1.0, right)
            dx[0] = jnp.broadcast_to(left, (8, WINDOW))
            dx[blocks + 1] = jnp.broadcast_to(right, (8, WINDOW))

        attend_block(jnp.where(tp < 2, half + i, half - 1 - i))
        return carry

    lax.fori_loop(0, half, far_step, 0)
    far_copy = remote(att.at[mate_across], am_far, ms.at[1], mr.at[1], {"tp": mate})
    far_copy.start()
    w_copy.wait_recv()
    far_copy.wait_recv()
    sent = []
    for c in range(chunks):
        cols = slice(c * cw, (c + 1) * cw)
        part = jnp.dot(att[across], w_ref[:, cols], preferred_element_type=f32)
        part += jnp.dot(am_far[...], w_mate[:, cols], preferred_element_type=f32)
        ysend[c] = part.astype(bf)
        copy = remote(ysend.at[c], yrecv.at[c], ys.at[c], yr.at[c], {"tp": across})
        copy.start()
        sent.append(copy)

    def near_step(i, carry):
        attend_block(jnp.where(tp < 2, half - 1 - i, half + i))
        return carry

    lax.fori_loop(0, half, near_step, 0)
    near_copy = remote(att.at[mate], am_near, ms.at[2], mr.at[2], {"tp": mate})
    near_copy.start()
    near_copy.wait_recv()
    for c in range(chunks):
        cols = slice(c * cw, (c + 1) * cw)
        part = jnp.dot(att[tp], w_ref[:, cols], preferred_element_type=f32)
        part += jnp.dot(am_near[...], w_mate[:, cols], preferred_element_type=f32)
        acc[:, cols] = part + res_ref[:, cols].astype(f32)
    for c in range(chunks):
        cols = slice(c * cw, (c + 1) * cw)
        sent[c].wait_recv()
        out_ref[:, cols] = (acc[:, cols] + yrecv[c].astype(f32)).astype(bf)
        if emit is not None:
            emit(c)
    for copy in halo + [w_copy, far_copy, near_copy] + sent:
        copy.wait_send()


def front_scratch(queries, key_rows, residual, out_weight):
    rows, width = residual.shape
    local, heads_width = queries.shape
    kv_width = key_rows.shape[1]
    blocks = local // WINDOW
    bf, f32 = jnp.bfloat16, jnp.float32
    dma = pltpu.SemaphoreType.DMA
    return [
            pltpu.VMEM((blocks + 2, WINDOW, kv_width), bf),
            pltpu.VMEM((blocks + 2, WINDOW, kv_width), bf),
            pltpu.VMEM((blocks, WINDOW), jnp.int32),
            pltpu.VMEM((blocks, WINDOW), jnp.int32),
            pltpu.VMEM((blocks + 2, 8, WINDOW), f32),
            pltpu.VMEM((4, rows, heads_width), bf),
            pltpu.VMEM((rows, heads_width), bf),
            pltpu.VMEM((rows, heads_width), bf),
            pltpu.VMEM(out_weight.shape, bf),
            pltpu.VMEM((rows, width), f32),
            pltpu.VMEM((CHUNKS, rows, width // CHUNKS), bf),
            pltpu.VMEM((CHUNKS, rows, width // CHUNKS), bf),
            dma((6,)), dma((6,)), dma((3,)), dma((3,)), dma((CHUNKS,)), dma((CHUNKS,)),
    ]


def front(queries, key_rows, value_rows, doc_ids, sink_logit, residual, out_weight):
    rows, width = residual.shape
    local, heads_width = queries.shape
    kv_width = key_rows.shape[1]
    blocks = local // WINDOW
    bf, f32 = jnp.bfloat16, jnp.float32
    dma = pltpu.SemaphoreType.DMA
    vm = pl.BlockSpec(memory_space=pltpu.VMEM)
    docs = doc_ids.reshape(blocks, WINDOW)
    return pl.pallas_call(
        functools.partial(front_kernel, CHUNKS, 0, None, None),
        out_shape=jax.ShapeDtypeStruct((rows, width), bf),
        in_specs=[pl.BlockSpec(memory_space=pltpu.SMEM)] + [vm] * 6,
        out_specs=vm,
        scratch_shapes=front_scratch(queries, key_rows, residual, out_weight),
        compiler_params=pltpu.CompilerParams(
            collective_id=4, has_side_effects=True, vmem_limit_bytes=48 * 1024 * 1024
        ),
        name="front",
    )(sink_logit, queries, key_rows, value_rows, docs, residual, out_weight)


def pair_routed(routes, gate_weight):
    count = lax.axis_size("sp")
    experts = count * gate_weight.shape[0]
    return (
        gate_weight.shape[0] == 1
        and routes.shape[1] == 2
        and experts == 2 * GROUPS
    )


def mixture(
    queries, key_rows, value_rows, doc_ids, sink_logit, residual, out_weight,
    norm_gain, routes, route_weights, gate_weight, up_weight, down_weight,
):
    rows, width = residual.shape
    docs = doc_ids.reshape(queries.shape[0] // WINDOW, WINDOW)
    ff = gate_weight.shape[2]
    groups = lax.axis_size("sp") // 2
    cap, cw = rows // groups, width // CHUNKS
    bf, f32 = jnp.bfloat16, jnp.float32
    quad = pltpu.VMEM((CHUNKS, groups, cap, cw), bf)
    flat = pltpu.VMEM((CHUNKS, rows, cw), bf)
    dma = pltpu.SemaphoreType.DMA
    vm = pl.BlockSpec(memory_space=pltpu.VMEM)
    hbm = pl.BlockSpec(memory_space=pl.ANY)
    return pl.pallas_call(
        functools.partial(moe_kernel, groups, CHUNKS),
        out_shape=jax.ShapeDtypeStruct((rows, width), bf),
        in_specs=[pl.BlockSpec(memory_space=pltpu.SMEM)] + [vm] * 9 + [hbm] * 3,
        out_specs=vm,
        scratch_shapes=front_scratch(queries, key_rows, residual, out_weight) + [
            pltpu.VMEM((rows, width), bf),
            quad, quad, quad, flat, flat, quad, quad,
            pltpu.VMEM((2, 8, rows), f32),
            pltpu.VMEM((groups, 2, 8, rows), f32),
            pltpu.VMEM((groups, 2, 8, rows), f32),
            pltpu.VMEM((width, ff), bf), pltpu.VMEM((width, ff), bf), pltpu.VMEM((ff, width), bf),
            pltpu.VMEM((2 * rows, ff), f32), pltpu.VMEM((2 * rows, ff), f32),
            dma((CHUNKS, groups)), dma((CHUNKS, groups)), dma((CHUNKS, groups)), dma((CHUNKS, groups)),
            dma((groups,)), dma((groups,)), dma((groups,)), dma((groups,)),
            dma((CHUNKS, groups)), dma((CHUNKS, groups)), dma((CHUNKS,)), dma((CHUNKS,)),
            dma((3,)),
        ],
        compiler_params=pltpu.CompilerParams(
            collective_id=3, has_side_effects=True, vmem_limit_bytes=56 * 1024 * 1024
        ),
        name="mixture",
    )(
        sink_logit, queries, key_rows, value_rows, docs, residual, out_weight,
        norm_gain[None, :], routes, route_weights, gate_weight, up_weight, down_weight,
    )


def fits_front(queries):
    return lax.axis_size("tp") == 4 and queries.shape[0] % (8 * WINDOW) == 0


def stream_of(
    queries, key_rows, value_rows, doc_ids, sink_logit, residual, out_weight
):
    local_rows = queries.shape[0]
    if fits_front(queries):
        return front(queries, key_rows, value_rows, doc_ids, sink_logit, residual, out_weight)
    anchor = lax.axis_index("sp") * local_rows
    extent = local_rows * lax.axis_size("sp")
    doc_float = doc_ids.astype(jnp.bfloat16)
    block_rows = min(512, local_rows)
    padded_keys, padded_values, padded_docs = fetch_margins(key_rows, value_rows, doc_float)
    block_parts = []
    for row_start in range(0, local_rows, block_rows):
        key_end = row_start + block_rows + 2 * WINDOW
        block_parts.append(
            attend(
                queries[row_start : row_start + block_rows],
                padded_keys[row_start:key_end],
                padded_values[row_start:key_end],
                doc_float[row_start : row_start + block_rows],
                padded_docs[row_start:key_end],
                anchor + row_start,
                anchor + row_start - WINDOW,
                sink_logit,
                extent,
            )
        )
    attended = jnp.concatenate(block_parts, axis=0)
    regrouped = lax.all_to_all(attended, "tp", split_axis=0, concat_axis=1, tiled=True)
    shard_rows = out_weight.shape[0]
    initial = jnp.zeros((regrouped.shape[0], out_weight.shape[1]), jnp.float32)
    running = initial
    weight_piece = lax.all_gather(out_weight, "tp", axis=0, tiled=True)
    for shard_index in range(weight_piece.shape[0] // shard_rows):
        columns = lax.dynamic_slice_in_dim(regrouped, shard_index * shard_rows, shard_rows, 1)
        partial_value = jnp.dot(
            columns,
            weight_piece[shard_index * shard_rows : (shard_index + 1) * shard_rows],
            preferred_element_type=jnp.float32,
        )
        running = running + partial_value.astype(jnp.bfloat16).astype(jnp.float32)
    stream = (residual.astype(jnp.float32) + running).astype(jnp.bfloat16)
    return stream


def per_device(
    queries,
    key_rows,
    value_rows,
    doc_ids,
    sink_logit,
    residual,
    out_weight,
    norm_gain,
    gate_weight,
    up_weight,
    down_weight,
    routes,
    route_weights,
):
    front_args = (
        queries, key_rows, value_rows, doc_ids, sink_logit, residual, out_weight
    )
    if pair_routed(routes, gate_weight) and fits_front(queries):
        return mixture(
            *front_args, norm_gain, routes, route_weights, gate_weight, up_weight, down_weight
        )
    stream = stream_of(*front_args)
    stream_f = stream.astype(jnp.float32)
    scale = lax.rsqrt(jnp.mean(stream_f * stream_f, axis=1, keepdims=True) + eps_norm)
    normed = (stream_f * scale * norm_gain[None, :]).astype(jnp.bfloat16)
    home_rows = normed.shape[0]
    width = normed.shape[1]
    route_count = routes.shape[1]
    expert_count = lax.axis_size("sp") * gate_weight.shape[0]
    capacity = route_count * home_rows // expert_count
    flat_routes = routes.reshape(-1)
    one_hot = (flat_routes[:, None] == jnp.arange(expert_count, dtype=jnp.int32)[None, :]).astype(
        jnp.int32
    )
    earlier = jnp.cumsum(one_hot, axis=0) - one_hot
    slot_rank = jnp.sum(earlier * one_hot, axis=1)
    slot_index = flat_routes * capacity + slot_rank
    source_row = (
        jnp.zeros((expert_count * capacity,), jnp.int32)
        .at[slot_index]
        .set(jnp.arange(home_rows * route_count, dtype=jnp.int32) // route_count)
    )
    outgoing = normed[source_row].reshape(expert_count, capacity, width)
    incoming = lax.all_to_all(outgoing, "sp", split_axis=0, concat_axis=0, tiled=True)
    flat_rows = incoming.reshape(-1, width)
    gate_act = jnp.dot(flat_rows, gate_weight[0], preferred_element_type=jnp.float32)
    up_act = jnp.dot(flat_rows, up_weight[0], preferred_element_type=jnp.float32)
    hidden = (jax.nn.silu(gate_act) * up_act).astype(jnp.bfloat16)
    produced = jnp.dot(hidden, down_weight[0], preferred_element_type=jnp.float32).astype(
        jnp.bfloat16
    )
    returned = lax.all_to_all(
        produced.reshape(incoming.shape), "sp", split_axis=0, concat_axis=0, tiled=True
    )
    route_out = returned.reshape(-1, width)[slot_index].reshape(home_rows, route_count, width)
    weighted = jnp.sum(route_weights[:, :, None] * route_out.astype(jnp.float32), axis=1)
    return (stream_f + weighted).astype(jnp.bfloat16)


def solution(mesh):
    return jax.shard_map(
        per_device,
        mesh=mesh,
        in_specs=(
            P("sp", "tp"),
            P("sp", "tp"),
            P("sp", "tp"),
            P("sp"),
            P("tp"),
            P(("sp", "tp"), None),
            P("tp", None),
            P(),
            P("sp", None, None),
            P("sp", None, None),
            P("sp", None, None),
            P(("sp", "tp"), None),
            P(("sp", "tp"), None),
        ),
        out_specs=P(("sp", "tp"), None),
        check_vma=False,
    )
```

profile of v0, /device:TPU:0, one launch (start us, length us, event | category | flops | bytes accessed | tf_op | source)
XLA Modules:
  0.0 100.6 jit_solution(4968626177159026836)
XLA Ops:
  0.0 1.5 %copy.14.routes_ref = s32[256,2]{1,0:T(8,128)} copy(s32[256,2]{0,1:T(2,128)} %param.24) | data formatting | bytes 4096 | tf_op args[11]
  1.5 1.5 %copy.15.rw_ref = f32[256,2]{1,0:T(8,128)} copy(f32[256,2]{0,1:T(2,128)} %param.25) | data formatting | bytes 4096 | tf_op args[12]
  2.9 95.3 %mixture.1 = bf16[256,2048]{1,0:T(8,128)(2,1)} custom-call(f32[8]{0:T(128)} %sink_ref.1, bf16[1024,512]{1,0:T(8,128)(2,1)} %q_ref.1, bf16[1024,128]{1,0:T(8,128)(2,1)} %k_ref.1, bf16[1024,128]{1,0:T(8,128)(2,1)} %v_ref.1, s32[8,128]{1,0:T(8,128)} %bitcast.3, bf16[256,2048]{1,0:T(8,128)(2,1)} %res_ref.1, bf16[512,2048]{1,0:T(8,128)(2,1)} %w_ref.1, ...), custom_call_target="tpu_custom_call" | custom-call | tf_op jit(solution)/shard_map/mixture/pallas_call | solution.py:501
  98.3 2.3 %copy.17 = bf16[256,2048]{1,0:T(8,128)(2,1)} copy(bf16[256,2048]{1,0:T(8,128)(2,1)} %mixture.1) | data formatting | bytes 2097152
where the time goes:
time: 101 us
  Pallas kernels  95.3 us (94%)
  local copies, waits for them, and re-layouts  5.24 us (5%)
    pallas_call x1, Pallas kernels, mixture(): pl.pallas_call(functools.partial(moe_kernel, groups, CHUNKS), out_shape=j...  95.3 us
    unnamed x3, local copies, waits for them, and re-layouts  5.24 us

commit v1 on v0

--- a/solution.py
+++ b/solution.py
@@ -11,6 +11,7 @@
 WINDOW = 128
 GROUPS = 4
 CHUNKS = 4
+HALVES = 2
 
 
 neg_fill = -1e30
@@ -79,205 +80,369 @@
     )
 
 
+def plane_order(gz):
+    return [(gz + 2) % 4, gz, 3 - gz, gz + 1 - 2 * (gz % 2)]
+
+
+def slots_of(routes, order, cap):
+    rows = routes.shape[1]
+    f32, bf = jnp.float32, jnp.bfloat16
+    group_of = routes[0:1, :] // 2
+    sub = lax.broadcasted_iota(jnp.int32, (8, rows), 0)
+    wanted = jnp.full((8, rows), -1, jnp.int32)
+    for k, plane in enumerate(order):
+        wanted = jnp.where(sub == k, plane, wanted)
+    one_hot = jnp.where(group_of == wanted, 1.0, 0.0)
+    ri = lax.broadcasted_iota(jnp.int32, (rows, rows), 0)
+    ci = lax.broadcasted_iota(jnp.int32, (rows, rows), 1)
+    above = jnp.where(ri < ci, 1.0, 0.0).astype(bf)
+    ranks = jnp.dot(one_hot.astype(bf), above, preferred_element_type=f32)
+    base = sub.astype(f32) * cap
+    return jnp.sum((ranks + base) * one_hot, axis=0, keepdims=True)
+
+
 def moe_kernel(
-    groups, chunks,
-    sink_ref, q_ref, k_ref, v_ref, doc_ref, res_ref, w_ref,
-    gain_ref, routes_ref, rw_ref, gate_hbm, up_hbm, down_hbm,
+    groups, halves,
+    sink_ref, doc_ref, routes_ref, rw_ref, gain_ref,
+    q_hbm, k_hbm, v_hbm, res_hbm, w_hbm, gate_hbm, up_hbm, down_hbm,
     out_ref,
-    kx, vx, dl, dr, dx, att, am_far, am_near, w_mate, acc, ysend, yrecv,
-    hs, hr, ms, mr, ys, yr,
-    stream_ref, send, own, peer, pout, pin, comb, ret, wsend, wown, wpeer,
-    gv, uv, dv, acc_g, acc_u,
-    zs, zr, xs, xr, zws, zwr, xws, xwr, bzs, bzr, bxs, bxr, wsem,
+    qv, resv, wv, w_mate, kx, vx, dl, dr, dx, att, am_far, am_near, routes_far,
+    mixed_att, acc, ysend, yrecv, send, own, peer, comb, ret, hid_own, hid_send, hid_recv,
+    wsend, wrecv, fin, gv, uv, dv, dv_mate,
+    ls, hs, hr, ms, mr, ys, yr, zs, zr, xs, xr, gs, gr, bs, br, ws, wr, ds, dr_sem,
 ):
-    me = lax.axis_index("sp")
-    gz = me // 2
-    side = me % 2
-    mate = gz * 2 + 1 - side
-    rows, width = res_ref.shape
+    sp = lax.axis_index("sp")
+    tp = lax.axis_index("tp")
+    sp_count = lax.axis_size("sp")
+    gz, side = sp // 2, sp % 2
+    x_mate = {"sp": gz * 2 + 1 - side}
+    mate = tp + 1 - 2 * (tp % 2)
+    core = tp % 2
+    across = (tp + 2) % 4
+    mate_across = (mate + 2) % 4
+    after = (sp + 1) % sp_count
+    before = (sp + sp_count - 1) % sp_count
+    order = plane_order(gz)
+    here = 1
+    away = [k for k in range(groups) if k != here]
+    rows, width = out_ref.shape
     cap = rows // groups
-    cw = width // chunks
-    half = groups // 2
-    offsets = [half] + [d for d in range(groups - 1, 0, -1) if d != half]
-
-    def remote(src, dst, ss, rs, target):
+    hw = width // halves
+    cw = width // 4
+    blocks = k_hbm.shape[0]
+    home_blocks = blocks // 4
+    half = blocks // 2
+    kv_heads = k_hbm.shape[2] // HD
+    ratio = q_hbm.shape[1] // k_hbm.shape[2]
+    heads = q_hbm.shape[1]
+    f32, bf = jnp.float32, jnp.bfloat16
+    mesh_id = pl.DeviceIdType.MESH
+
+    def remote(src, dst, s_sem, r_sem, where):
         return pltpu.make_async_remote_copy(
-            src_ref=src, dst_ref=dst, send_sem=ss, recv_sem=rs,
-            device_id={"sp": target}, device_id_type=pl.DeviceIdType.MESH,
+            src_ref=src, dst_ref=dst, send_sem=s_sem, recv_sem=r_sem,
+            device_id=where, device_id_type=mesh_id,
         )
 
+    def to_plane(k):
+        return {"sp": order[k] * 2 + side}
+
     barrier = pltpu.get_barrier_semaphore()
-    for d in offsets:
-        pl.semaphore_signal(
-            barrier, inc=1, device_id={"sp": ((gz + d) % groups) * 2 + side},
-            device_id_type=pl.DeviceIdType.MESH,
-        )
-    pl.semaphore_signal(
-        barrier, inc=1, device_id={"sp": mate}, device_id_type=pl.DeviceIdType.MESH
-    )
+    partners = [{"sp": after}, {"sp": before}, {"tp": mate}, {"tp": across}, x_mate]
+    partners += [to_plane(k) for k in away]
+    for where in partners:
+        pl.semaphore_signal(barrier, inc=1, device_id=where, device_id_type=mesh_id)
     loads = [
-        pltpu.make_async_copy(s.at[0], t, wsem.at[i])
-        for i, (s, t) in enumerate(((gate_hbm, gv), (up_hbm, uv), (down_hbm, dv)))
+        pltpu.make_async_copy(src, dst, ls.at[i])
+        for i, (src, dst) in enumerate((
+            (k_hbm, kx.at[pl.ds(1, blocks)]), (v_hbm, vx.at[pl.ds(1, blocks)]), (q_hbm, qv),
+            (w_hbm, wv), (res_hbm, resv), (gate_hbm.at[0], gv), (up_hbm.at[0], uv),
+            (down_hbm.at[0], dv),
+        ))
     ]
     for load in loads:
         load.start()
-
-    first = routes_ref[:, 0:1]
-    group_of = first // 2
-    lanes = lax.broadcasted_iota(jnp.int32, (rows, 128), 1)
-    one_hot = jnp.where(group_of == lanes, 1.0, 0.0)
+    for b in range(blocks):
+        dx[b + 1] = jnp.broadcast_to(doc_ref[b:b + 1, :].astype(f32), (8, WINDOW))
+
+    slot = slots_of(routes_ref[...], order, cap)
     ri = lax.broadcasted_iota(jnp.int32, (rows, rows), 0)
     ci = lax.broadcasted_iota(jnp.int32, (rows, rows), 1)
-    below = jnp.where(ci < ri, 1.0, 0.0).astype(jnp.bfloat16)
-    ranks = jnp.dot(below, one_hot.astype(jnp.bfloat16), preferred_element_type=jnp.float32)
-    slot = group_of.astype(jnp.float32) * cap + jnp.sum(ranks * one_hot, axis=1, keepdims=True)
-    spread = jnp.where(slot == ci.astype(jnp.float32), 1.0, 0.0)
-    spread_b = spread.astype(jnp.bfloat16)
-    slot_lane = jnp.sum(jnp.where(ri == ci, slot, 0.0), axis=0, keepdims=True)
-    pick = jnp.where(ri.astype(jnp.float32) == slot_lane, 1.0, 0.0).astype(jnp.bfloat16)
-    for parity in range(2):
-        w_col = jnp.where(first % 2 == parity, rw_ref[:, 0:1], rw_ref[:, 1:2])
-        w_row = jnp.sum(spread * w_col, axis=0, keepdims=True)
-        wsend[parity] = jnp.broadcast_to(w_row, (8, rows))
-
+    slot_col = jnp.sum(jnp.where(ri == ci, slot, 0.0), axis=1, keepdims=True)
+    spread = jnp.where(slot_col == ci.astype(f32), 1.0, 0.0)
+    weight_rows = []
+    for parity in (side, 1 - side):
+        w_row = jnp.where(routes_ref[0:1, :] % 2 == parity, rw_ref[0:1, :], rw_ref[1:2, :])
+        w_col = jnp.sum(jnp.where(ri == ci, w_row, 0.0), axis=1, keepdims=True)
+        weight_rows.append(jnp.sum(spread * w_col, axis=0, keepdims=True))
+    sub8 = lax.broadcasted_iota(jnp.int32, (8, rows), 0)
+    wsend[...] = jnp.where(
+        sub8 == 0, weight_rows[0], jnp.where(sub8 == 1, weight_rows[1], 0.0)
+    )
+
+    loads[0].wait()
+    loads[1].wait()
+    pl.semaphore_wait(barrier, len(partners))
     pending = []
 
-    def entered():
-        for d in offsets:
-            copy = remote(
-                wsend, wown.at[gz], zws.at[d], zwr.at[gz], ((gz + d) % groups) * 2 + side
-            )
-            copy.start()
-            pending.append(copy)
-        copy = remote(wsend, wpeer.at[gz], xws.at[gz], xwr.at[gz], mate)
+    def go(copy):
         copy.start()
         pending.append(copy)
-
-    def emit(j):
-        rows_j = stream_ref[:, j * cw:(j + 1) * cw]
-        piece = jnp.dot(pick, rows_j, preferred_element_type=jnp.float32)
-        send[j] = piece.astype(jnp.bfloat16).reshape(groups, cap, cw)
-        for d in offsets:
-            target = (gz + d) % groups
-            copy = remote(
-                send.at[j, target], own.at[j, gz], zs.at[j, d], zr.at[j, gz], target * 2 + side
+        return copy
+
+    halo = [
+        go(remote(src, dst, hs.at[i], hr.at[i], {"sp": where}))
+        for i, (src, dst, where) in enumerate((
+            (kx.at[blocks], kx.at[0], after), (vx.at[blocks], vx.at[0], after),
+            (doc_ref, dl, after),
+            (kx.at[1], kx.at[blocks + 1], before), (vx.at[1], vx.at[blocks + 1], before),
+            (doc_ref, dr, before),
+        ))
+    ]
+    w_copy = go(remote(w_hbm, w_mate, ms.at[0], mr.at[0], {"tp": mate}))
+    r_copy = go(remote(routes_ref, routes_far, ms.at[3], mr.at[3], {"tp": across}))
+    for k in away:
+        go(remote(wsend, wrecv.at[k], ws.at[k], wr.at[k], to_plane(k)))
+    ff = dv.shape[0]
+    own_half = pl.ds(core * (ff // 2), ff // 2)
+    d_copy = go(remote(down_hbm.at[0, own_half], dv_mate.at[own_half], ds.at[0], dr_sem.at[0], x_mate))
+
+    qi = lax.broadcasted_iota(jnp.int32, (WINDOW, 3 * WINDOW), 0)
+    ki = lax.broadcasted_iota(jnp.int32, (WINDOW, 3 * WINDOW), 1)
+    band = (ki >= qi) & (ki <= qi + 2 * WINDOW)
+    eye = lax.broadcasted_iota(jnp.int32, (WINDOW, WINDOW), 0) == lax.broadcasted_iota(
+        jnp.int32, (WINDOW, WINDOW), 1
+    )
+
+    def attend_block(b):
+        own_docs = dx[b + 1][0:1]
+        key_docs = jnp.concatenate([dx[b][0:1], own_docs, dx[b + 2][0:1]], axis=1)
+        query_docs = jnp.sum(jnp.where(eye, own_docs, 0.0), axis=1, keepdims=True)
+        bias = jnp.where(band & (key_docs == query_docs), 0.0, neg_fill)
+        keys = kx[pl.ds(b, 3)].reshape(3 * WINDOW, kv_heads * HD)
+        values = vx[pl.ds(b, 3)].reshape(3 * WINDOW, kv_heads * HD)
+        home = b // home_blocks
+        to_rows = pl.ds(pl.multiple_of((b % home_blocks) * WINDOW, WINDOW), WINDOW)
+        from_rows = pl.ds(pl.multiple_of(b * WINDOW, WINDOW), WINDOW)
+        for g in range(kv_heads):
+            span = slice(g * ratio * HD, (g + 1) * ratio * HD)
+            q = qv[from_rows, span] * jnp.asarray(HD ** (-0.5), bf)
+            stacked = jnp.concatenate([q[:, r * HD:(r + 1) * HD] for r in range(ratio)], axis=0)
+            scores = lax.dot_general(
+                stacked, keys[:, g * HD:(g + 1) * HD], (((1,), (1,)), ((), ())),
+                preferred_element_type=f32,
             )
-            copy.start()
-            pending.append(copy)
-        copy = remote(send.at[j, gz], peer.at[j, gz], xs.at[j, gz], xr.at[j, gz], mate)
-        copy.start()
-        pending.append(copy)
-        own[j, pl.ds(gz, 1)] = send[j, pl.ds(gz, 1)]
-
-    front_kernel(
-        chunks, groups, entered, emit,
-        sink_ref, q_ref, k_ref, v_ref, doc_ref, res_ref, w_ref,
-        stream_ref,
-        kx, vx, dl, dr, dx, att, am_far, am_near, w_mate, acc, ysend, yrecv,
-        hs, hr, ms, mr, ys, yr,
-    )
-    wown[pl.ds(gz, 1)] = wsend[...][None]
-
-    for d in offsets:
-        source = (gz + groups - d) % groups
-        remote(wsend, wown.at[source], zws.at[d], zwr.at[source], mate).wait_recv()
-        copy = remote(wown.at[source], wpeer.at[source], xws.at[source], xwr.at[source], mate)
-        copy.start()
-        pending.append(copy)
-
-    loads[0].wait()
-    loads[1].wait()
-
-    squares = {0: 0.0, rows: 0.0}
-
-    def accumulate(buf, j, base):
-        wide = buf[j].reshape(rows, cw).astype(jnp.float32)
-        squares[base] = squares[base] + jnp.sum(wide * wide, axis=1, keepdims=True)
-        block = (wide * gain_ref[:, j * cw:(j + 1) * cw]).astype(jnp.bfloat16)
-        part_g = jnp.dot(block, gv[j * cw:(j + 1) * cw, :], preferred_element_type=jnp.float32)
-        part_u = jnp.dot(block, uv[j * cw:(j + 1) * cw, :], preferred_element_type=jnp.float32)
-        if j == 0:
-            acc_g[base:base + rows, :] = part_g
-            acc_u[base:base + rows, :] = part_u
+            vg = values[:, g * HD:(g + 1) * HD]
+            parts = []
+            for r in range(ratio):
+                sink = sink_ref[g * ratio + r]
+                s = scores[r * WINDOW:(r + 1) * WINDOW] + bias
+                top = jnp.maximum(jnp.max(s, axis=1, keepdims=True), sink)
+                e = jnp.exp(s - top)
+                den = jnp.sum(e, axis=1, keepdims=True) + jnp.exp(sink - top)
+                o = jnp.dot(e.astype(bf), vg, preferred_element_type=f32)
+                parts.append((o / den).astype(bf))
+            att[home, to_rows, span] = jnp.concatenate(parts, axis=1)
+
+    def far_step(i, carry):
+        @pl.when(i == half - 1)
+        def _():
+            for copy in halo:
+                copy.wait_recv()
+            left = dl[blocks - 1:blocks, :].astype(f32)
+            right = dr[0:1, :].astype(f32)
+            left = jnp.where(sp == 0, -1.0, left)
+            right = jnp.where(sp == sp_count - 1, -1.0, right)
+            dx[0] = jnp.broadcast_to(left, (8, WINDOW))
+            dx[blocks + 1] = jnp.broadcast_to(right, (8, WINDOW))
+
+        attend_block(jnp.where(tp < 2, half + i, half - 1 - i))
+        return carry
+
+    def pick_of(slot_row):
+        return jnp.where(ri.astype(f32) == slot_row, 1.0, 0.0).astype(bf)
+
+    def gather_rows(pick, mine, mates):
+        mixed_att[:, :heads] = jnp.dot(pick, mine, preferred_element_type=f32).astype(bf)
+        mixed_att[:, heads:] = jnp.dot(pick, mates, preferred_element_type=f32).astype(bf)
+
+    def project(cols):
+        part = jnp.dot(mixed_att[:, :heads], wv[:, cols], preferred_element_type=f32)
+        return part + jnp.dot(mixed_att[:, heads:], w_mate[:, cols], preferred_element_type=f32)
+
+    loads[2].wait()
+    with jax.named_scope("attn_far"):
+        lax.fori_loop(0, half, far_step, 0)
+    far_copy = go(remote(att.at[mate_across], am_far, ms.at[1], mr.at[1], {"tp": mate}))
+    with jax.named_scope("wait_far"):
+        r_copy.wait_recv()
+        pick_far = pick_of(slots_of(routes_far[...], order, cap))
+        loads[3].wait()
+        w_copy.wait_recv()
+        far_copy.wait_recv()
+    with jax.named_scope("far_proj"):
+        gather_rows(pick_far, att[across], am_far[...])
+        y_copies = {}
+
+        def send_y(k, h):
+            y_copies[k, h] = go(remote(
+                ysend.at[h, k], yrecv.at[h, k], ys.at[h, k], yr.at[h, k], {"tp": across}
+            ))
+
+        per = 4 // halves
+        for h in range(halves):
+            for c in range(per):
+                cols = slice(h * hw + c * cw, h * hw + (c + 1) * cw)
+                part = project(cols).astype(bf).reshape(groups, cap, cw)
+                ysend[h, :, :, c * cw:(c + 1) * cw] = part
+            if h < halves - 1:
+                send_y(0, h)
+        send_y(0, halves - 1)
+        for k in range(1, groups):
+            for h in range(halves):
+                send_y(k, h)
+
+    def near_step(i, carry):
+        attend_block(jnp.where(tp < 2, half - 1 - i, half + i))
+        return carry
+
+    with jax.named_scope("attn_near"):
+        lax.fori_loop(0, half, near_step, 0)
+    near_copy = go(remote(att.at[mate], am_near, ms.at[2], mr.at[2], {"tp": mate}))
+    for i in range(4, 8):
+        loads[i].wait()
+    with jax.named_scope("wait_near"):
+        pick = pick_of(slot)
+        near_copy.wait_recv()
+    with jax.named_scope("near_proj"):
+        gather_rows(pick, att[tp], am_near[...])
+        for c in range(4):
+            cols = slice(c * cw, (c + 1) * cw)
+            part = project(cols)
+            part += jnp.dot(pick, resv[:, cols], preferred_element_type=f32)
+            acc[:, :, cols] = part.reshape(groups, cap, cw)
+
+    def emit(k, h):
+        with jax.named_scope("y%d_%d" % (k, h)):
+            y_copies[k, h].wait_recv()
+        cols = slice(h * hw, (h + 1) * hw)
+        piece = (acc[k, :, cols] + yrecv[h, k].astype(f32)).astype(bf)
+        send[h, k] = piece
+        if k == here:
+            own[h, k] = piece
+            go(remote(send.at[h, k], peer.at[h, k], xs.at[h, k], xr.at[h, k], x_mate))
         else:
-            acc_g[base:base + rows, :] += part_g
-            acc_u[base:base + rows, :] += part_u
-
-    def peer_step(j):
-        for s in range(groups):
-            remote(send.at[j, s], peer.at[j, s], xs.at[j, s], xr.at[j, s], mate).wait_recv()
-        accumulate(peer, j, rows)
-
-    for j in range(chunks):
-        for d in offsets:
-            source = (gz + groups - d) % groups
-            remote(
-                send.at[j, source], own.at[j, source], zs.at[j, d], zr.at[j, source], mate
-            ).wait_recv()
-            copy = remote(
-                own.at[j, source], peer.at[j, source], xs.at[j, source], xr.at[j, source], mate
-            )
-            copy.start()
-            pending.append(copy)
-        accumulate(own, j, 0)
-        if j:
-            peer_step(j - 1)
-    peer_step(chunks - 1)
-    for s in range(groups):
-        remote(wsend, wpeer.at[s], xws.at[s], xwr.at[s], mate).wait_recv()
-
-    def hidden_of(base):
-        scale = lax.rsqrt(squares[base] / width + eps_norm)
-        g = acc_g[base:base + rows, :] * scale
-        u = acc_u[base:base + rows, :] * scale
-        return (g / (1.0 + jnp.exp(-g)) * u).astype(jnp.bfloat16)
-
-    sub = lax.broadcasted_iota(jnp.int32, (cap, rows), 0)
-    lane = lax.broadcasted_iota(jnp.int32, (cap, rows), 1)
-    chosen = lane == sub + gz * cap
-
-    def weights_of(buf):
-        cols = []
-        for s in range(groups):
-            row = jnp.where(side == 0, buf[s, 0, 0:1, :], buf[s, 1, 0:1, :])
-            cols.append(jnp.sum(jnp.where(chosen, row, 0.0), axis=1, keepdims=True))
-        return jnp.concatenate(cols, axis=0)
-
-    w_peer = weights_of(wpeer)
-    hid_peer = hidden_of(rows)
-    loads[2].wait()
-    for j in range(chunks):
-        part = jnp.dot(hid_peer, dv[:, j * cw:(j + 1) * cw], preferred_element_type=jnp.float32)
-        pout[j] = (part * w_peer).astype(jnp.bfloat16)
-        copy = remote(pout.at[j], pin.at[j], bxs.at[j], bxr.at[j], mate)
-        copy.start()
-        pending.append(copy)
-    w_own = weights_of(wown)
-    hid_own = hidden_of(0)
-    for j in range(chunks):
-        part = jnp.dot(hid_own, dv[:, j * cw:(j + 1) * cw], preferred_element_type=jnp.float32)
-        remote(pout.at[j], pin.at[j], bxs.at[j], bxr.at[j], mate).wait_recv()
-        total = part * w_own + pin[j].astype(jnp.float32)
-        comb[j] = total.astype(jnp.bfloat16).reshape(groups, cap, cw)
-        for d in offsets:
-            target = (gz + d) % groups
-            copy = remote(
-                comb.at[j, target], ret.at[j, gz], bzs.at[j, d], bzr.at[j, gz], target * 2 + side
-            )
-            copy.start()
-            pending.append(copy)
-        ret[j, pl.ds(gz, 1)] = comb[j, pl.ds(gz, 1)]
-    for j in range(chunks):
-        for d in offsets:
-            source = (gz + groups - d) % groups
-            remote(
-                comb.at[j, source], ret.at[j, source], bzs.at[j, d], bzr.at[j, source], mate
-            ).wait_recv()
-        back = jnp.dot(spread_b, ret[j].reshape(rows, cw), preferred_element_type=jnp.float32)
-        cols = slice(j * cw, (j + 1) * cw)
-        out_ref[:, cols] = (stream_ref[:, cols].astype(jnp.float32) + back).astype(jnp.bfloat16)
-    for copy in pending:
-        copy.wait_send()
+            go(remote(send.at[h, k], own.at[h, k], zs.at[h, k], zr.at[h, k], to_plane(k)))
+
+    def relay(k, h):
+        with jax.named_scope("z%d_%d" % (k, h)):
+            remote(send.at[h, k], own.at[h, k], zs.at[h, k], zr.at[h, k], x_mate).wait_recv()
+        go(remote(own.at[h, k], peer.at[h, k], xs.at[h, k], xr.at[h, k], x_mate))
+
+    def hidden_of(buf, k):
+        squares = gate_act = up_act = 0.0
+        for h in range(halves):
+            span = slice(h * hw, (h + 1) * hw)
+            wide = buf[h, k].astype(f32)
+            squares = squares + jnp.sum(wide * wide, axis=1, keepdims=True)
+            block = (wide * gain_ref[:, span]).astype(bf)
+            gate_act = gate_act + jnp.dot(block, gv[span, :], preferred_element_type=f32)
+            up_act = up_act + jnp.dot(block, uv[span, :], preferred_element_type=f32)
+        scale = lax.rsqrt(squares / width + eps_norm)
+        g = gate_act * scale
+        return (g / (1.0 + jnp.exp(-g)) * (up_act * scale)).astype(bf)
+
+    def expert_own(k):
+        with jax.named_scope("own%d" % k):
+            hid_own[k] = hidden_of(own, k)
+
+    def expert_peer(k):
+        with jax.named_scope("x%d" % k):
+            for h in range(halves):
+                remote(own.at[h, k], peer.at[h, k], xs.at[h, k], xr.at[h, k], x_mate).wait_recv()
+        with jax.named_scope("peer%d" % k):
+            hid_send[k] = hidden_of(peer, k)
+            go(remote(hid_send.at[k], hid_recv.at[k], gs.at[k], gr.at[k], x_mate))
+
+    sub_c = lax.broadcasted_iota(jnp.int32, (cap, rows), 0)
+    lane_c = lax.broadcasted_iota(jnp.int32, (cap, rows), 1)
+
+    def combine(k):
+        with jax.named_scope("hid%d" % k):
+            remote(hid_send.at[k], hid_recv.at[k], gs.at[k], gr.at[k], x_mate).wait_recv()
+            if k == here:
+                table = wsend[...]
+            else:
+                remote(wsend, wrecv.at[k], ws.at[k], wr.at[k], x_mate).wait_recv()
+                table = wrecv[k]
+        with jax.named_scope("down%d" % k):
+            chosen = lane_c == sub_c + k * cap
+            w_own = jnp.sum(jnp.where(chosen, table[0:1, :], 0.0), axis=1, keepdims=True)
+            w_peer = jnp.sum(jnp.where(chosen, table[1:2, :], 0.0), axis=1, keepdims=True)
+            mine, theirs = hid_own[k], hid_recv[k]
+            for h in range(halves):
+                for c in range(per):
+                    cols = slice(h * hw + c * cw, h * hw + (c + 1) * cw)
+                    total = jnp.dot(mine, dv[:, cols], preferred_element_type=f32) * w_own
+                    total += jnp.dot(theirs, dv_mate[:, cols], preferred_element_type=f32) * w_peer
+                    comb[h, k, :, c * cw:(c + 1) * cw] = total.astype(bf)
+                if k != here:
+                    go(remote(comb.at[h, k], ret.at[h, k], bs.at[h, k], br.at[h, k], to_plane(k)))
+
+    def finish(k, h):
+        if k == here:
+            back = comb[h, k]
+        else:
+            with jax.named_scope("r%d_%d" % (k, h)):
+                remote(comb.at[h, k], ret.at[h, k], bs.at[h, k], br.at[h, k], x_mate).wait_recv()
+            back = ret[h, k]
+        total = send[h, k].astype(f32) + back.astype(f32)
+        fin[k * cap:(k + 1) * cap, h * hw:(h + 1) * hw] = total.astype(bf)
+
+    hs_all = range(halves)
+    for k in (0, here):
+        for h in hs_all:
+            emit(k, h)
+    with jax.named_scope("dmate"):
+        d_copy.wait_recv()
+    d_fwd = go(remote(
+        dv_mate.at[own_half], dv_mate.at[own_half], ds.at[1], dr_sem.at[1], {"tp": mate}
+    ))
+    expert_own(here)
+    for h in hs_all[:-1]:
+        relay(0, h)
+    for h in hs_all:
+        emit(2, h)
+    relay(0, halves - 1)
+    expert_own(0)
+    expert_peer(here)
+    for h in hs_all:
+        emit(3, h)
+    d_fwd.wait_recv()
+    combine(here)
+    expert_peer(0)
+    combine(0)
+    for k in (3, 2):
+        for h in hs_all:
+            relay(k, h)
+        expert_own(k)
+    for k in (3, 2):
+        expert_peer(k)
+    for k in (3, 2):
+        combine(k)
+    for k in (here, 0, 3, 2):
+        for h in hs_all:
+            finish(k, h)
+    with jax.named_scope("out"):
+        spread_b = spread.astype(bf)
+        for c in range(4):
+            cols = slice(c * cw, (c + 1) * cw)
+            out_ref[:, cols] = jnp.dot(
+                spread_b, fin[:, cols], preferred_element_type=f32
+            ).astype(bf)
+    with jax.named_scope("sends"):
+        for copy in pending:
+            copy.wait_send()
 
 
 def front_kernel(
@@ -488,41 +653,57 @@
     norm_gain, routes, route_weights, gate_weight, up_weight, down_weight,
 ):
     rows, width = residual.shape
-    docs = doc_ids.reshape(queries.shape[0] // WINDOW, WINDOW)
+    blocks = queries.shape[0] // WINDOW
+    heads = queries.shape[1]
+    kv_width = key_rows.shape[1]
+    docs = doc_ids.reshape(blocks, WINDOW)
     ff = gate_weight.shape[2]
     groups = lax.axis_size("sp") // 2
-    cap, cw = rows // groups, width // CHUNKS
-    bf, f32 = jnp.bfloat16, jnp.float32
-    quad = pltpu.VMEM((CHUNKS, groups, cap, cw), bf)
-    flat = pltpu.VMEM((CHUNKS, rows, cw), bf)
+    cap, hw = rows // groups, width // HALVES
+    bf, f32, i32 = jnp.bfloat16, jnp.float32, jnp.int32
+    pieces = pltpu.VMEM((HALVES, groups, cap, hw), bf)
+    hidden = pltpu.VMEM((groups, cap, ff), bf)
     dma = pltpu.SemaphoreType.DMA
     vm = pl.BlockSpec(memory_space=pltpu.VMEM)
     hbm = pl.BlockSpec(memory_space=pl.ANY)
+    edge = pltpu.VMEM((blocks + 2, WINDOW, kv_width), bf)
+    per_piece = dma((HALVES, groups))
     return pl.pallas_call(
-        functools.partial(moe_kernel, groups, CHUNKS),
+        functools.partial(moe_kernel, groups, HALVES),
         out_shape=jax.ShapeDtypeStruct((rows, width), bf),
-        in_specs=[pl.BlockSpec(memory_space=pltpu.SMEM)] + [vm] * 9 + [hbm] * 3,
+        in_specs=[pl.BlockSpec(memory_space=pltpu.SMEM)] + [vm] * 4 + [hbm] * 8,
         out_specs=vm,
-        scratch_shapes=front_scratch(queries, key_rows, residual, out_weight) + [
+        scratch_shapes=[
+            pltpu.VMEM(queries.shape, bf), pltpu.VMEM((rows, width), bf),
+            pltpu.VMEM(out_weight.shape, bf), pltpu.VMEM(out_weight.shape, bf),
+            edge, edge,
+            pltpu.VMEM((blocks, WINDOW), i32), pltpu.VMEM((blocks, WINDOW), i32),
+            pltpu.VMEM((blocks + 2, 8, WINDOW), f32),
+            pltpu.VMEM((4, rows, heads), bf),
+            pltpu.VMEM((rows, heads), bf), pltpu.VMEM((rows, heads), bf),
+            pltpu.VMEM(routes.shape[::-1], i32),
+            pltpu.VMEM((rows, 2 * heads), bf),
+            pltpu.VMEM((groups, cap, width), f32),
+            pieces, pieces, pieces, pieces, pieces, pieces, pieces,
+            hidden, hidden, hidden,
+            pltpu.VMEM((8, rows), f32), pltpu.VMEM((groups, 8, rows), f32),
             pltpu.VMEM((rows, width), bf),
-            quad, quad, quad, flat, flat, quad, quad,
-            pltpu.VMEM((2, 8, rows), f32),
-            pltpu.VMEM((groups, 2, 8, rows), f32),
-            pltpu.VMEM((groups, 2, 8, rows), f32),
-            pltpu.VMEM((width, ff), bf), pltpu.VMEM((width, ff), bf), pltpu.VMEM((ff, width), bf),
-            pltpu.VMEM((2 * rows, ff), f32), pltpu.VMEM((2 * rows, ff), f32),
-            dma((CHUNKS, groups)), dma((CHUNKS, groups)), dma((CHUNKS, groups)), dma((CHUNKS, groups)),
-            dma((groups,)), dma((groups,)), dma((groups,)), dma((groups,)),
-            dma((CHUNKS, groups)), dma((CHUNKS, groups)), dma((CHUNKS,)), dma((CHUNKS,)),
-            dma((3,)),
+            pltpu.VMEM((width, ff), bf), pltpu.VMEM((width, ff), bf),
+            pltpu.VMEM((ff, width), bf), pltpu.VMEM((ff, width), bf),
+            dma((8,)), dma((6,)), dma((6,)), dma((4,)), dma((4,)),
+            per_piece, per_piece, per_piece, per_piece, per_piece, per_piece,
+            dma((groups,)), dma((groups,)), per_piece, per_piece,
+            dma((groups,)), dma((groups,)), dma((2,)), dma((2,)),
         ],
         compiler_params=pltpu.CompilerParams(
             collective_id=3, has_side_effects=True, vmem_limit_bytes=56 * 1024 * 1024
         ),
         name="mixture",
     )(
-        sink_logit, queries, key_rows, value_rows, docs, residual, out_weight,
-        norm_gain[None, :], routes, route_weights, gate_weight, up_weight, down_weight,
+        sink_logit, docs, routes.T, route_weights.T, norm_gain[None, :],
+        queries, key_rows.reshape(blocks, WINDOW, kv_width),
+        value_rows.reshape(blocks, WINDOW, kv_width), residual, out_weight,
+        gate_weight, up_weight, down_weight,
     )
 
 

time: 101 us -> 82.5 us (0.82)
  Pallas kernels: 95.3 us -> 80 us
  local copies, waits for them, and re-layouts: 5.24 us -> 2.3 us
    pallas_call x1, Pallas kernels: 95.3 us -> 80 us  [mixture(): pl.pallas_call(functools.partial(moe_kernel, groups, HALVES), out_shape=j...]
    unnamed x3 -> x1, local copies, waits for them, and re-layouts: 5.24 us -> 2.3 us
where the time goes in v1:
time: 82.5 us; the launch traced here: 82.3 us
  Pallas kernels  80 us (97%)
  local copies, waits for them, and re-layouts  2.3 us (3%)
    pallas_call x1, Pallas kernels, mixture(): pl.pallas_call(functools.partial(moe_kernel, groups, HALVES), out_shape=j...  80 us
    unnamed x1, local copies, waits for them, and re-layouts  2.3 us

profile of v1, /device:TPU:0, one launch (start us, length us, event | category | flops | bytes accessed | tf_op | source)
XLA Modules:
  0.0 82.3 jit_solution(6870387408847553132)
XLA Ops:
  0.0 80.0 %mixture.1 = bf16[256,2048]{1,0:T(8,128)(2,1)} custom-call(f32[8]{0:T(128)} %sink_ref.1, s32[8,128]{1,0:T(8,128)} %bitcast.9, s32[2,256]{1,0:T(2,128)} %bitcast.10, f32[2,256]{1,0:T(2,128)} %bitcast.11, f32[1,2048]{1,0:T(1,128)} %bitcast.8, bf16[1024,512]{1,0:T(8,128)(2,1)} %q_hbm.1, bf16[8,128,128]{2,1,0:T(8,128)(2,1)} %bitcast.6, ...), custom_call_target="tpu_custom_call" | custom-call | tf_op jit(solution)/shard_map/mixture/pallas_call | solution.py:671
  80.0 2.3 %copy.15 = bf16[256,2048]{1,0:T(8,128)(2,1)} copy(bf16[256,2048]{1,0:T(8,128)(2,1)} %mixture.1) | data formatting | bytes 2097152

commit v2 on v1

--- a/solution.py
+++ b/solution.py
@@ -81,7 +81,7 @@
 
 
 def plane_order(gz):
-    return [(gz + 2) % 4, gz, 3 - gz, gz + 1 - 2 * (gz % 2)]
+    return [(gz + 2) % 4, 3 - gz, gz + 1 - 2 * (gz % 2), gz]
 
 
 def slots_of(routes, order, cap):
@@ -123,7 +123,7 @@
     after = (sp + 1) % sp_count
     before = (sp + sp_count - 1) % sp_count
     order = plane_order(gz)
-    here = 1
+    here = groups - 1
     away = [k for k in range(groups) if k != here]
     rows, width = out_ref.shape
     cap = rows // groups
@@ -144,8 +144,19 @@
             device_id=where, device_id_type=mesh_id,
         )
 
+    end = (gz == 0) | (gz == groups - 1)
+
+    def pick_one(at_end, at_middle):
+        return at_end if at_end == at_middle else jnp.where(end, at_end, at_middle)
+
+    emit_order = [pick_one(a, b) for a, b in ((0, 2), (1, 3), (2, 0), (3, 1))]
+    serve_order = [pick_one(a, b) for a, b in ((2, 0), (1, 3), (0, 2), (3, 1))]
+
     def to_plane(k):
-        return {"sp": order[k] * 2 + side}
+        plane = order[3]
+        for i in range(groups - 1):
+            plane = jnp.where(k == i, order[i], plane)
+        return {"sp": plane * 2 + side}
 
     barrier = pltpu.get_barrier_semaphore()
     partners = [{"sp": after}, {"sp": before}, {"tp": mate}, {"tp": across}, x_mate]
@@ -179,6 +190,8 @@
     wsend[...] = jnp.where(
         sub8 == 0, weight_rows[0], jnp.where(sub8 == 1, weight_rows[1], 0.0)
     )
+
+    wrecv[here] = wsend[...]
 
     loads[0].wait()
     loads[1].wait()
@@ -282,12 +295,11 @@
         far_copy.wait_recv()
     with jax.named_scope("far_proj"):
         gather_rows(pick_far, att[across], am_far[...])
-        y_copies = {}
-
-        def send_y(k, h):
-            y_copies[k, h] = go(remote(
+
+        def y_copy(k, h):
+            return remote(
                 ysend.at[h, k], yrecv.at[h, k], ys.at[h, k], yr.at[h, k], {"tp": across}
-            ))
+            )
 
         per = 4 // halves
         for h in range(halves):
@@ -296,11 +308,11 @@
                 part = project(cols).astype(bf).reshape(groups, cap, cw)
                 ysend[h, :, :, c * cw:(c + 1) * cw] = part
             if h < halves - 1:
-                send_y(0, h)
-        send_y(0, halves - 1)
-        for k in range(1, groups):
+                go(y_copy(emit_order[0], h))
+        go(y_copy(emit_order[0], halves - 1))
+        for k in emit_order[1:]:
             for h in range(halves):
-                send_y(k, h)
+                go(y_copy(k, h))
 
     def near_step(i, carry):
         attend_block(jnp.where(tp < 2, half - 1 - i, half + i))
@@ -314,36 +326,56 @@
     with jax.named_scope("wait_near"):
         pick = pick_of(slot)
         near_copy.wait_recv()
-    with jax.named_scope("near_proj"):
-        gather_rows(pick, att[tp], am_near[...])
-        for c in range(4):
-            cols = slice(c * cw, (c + 1) * cw)
-            part = project(cols)
-            part += jnp.dot(pick, resv[:, cols], preferred_element_type=f32)
-            acc[:, :, cols] = part.reshape(groups, cap, cw)
-
-    def emit(k, h):
-        with jax.named_scope("y%d_%d" % (k, h)):
-            y_copies[k, h].wait_recv()
+    def near_project(h):
+        with jax.named_scope("near_proj%d" % h):
+            for c in range(per):
+                cols = slice(h * hw + c * cw, h * hw + (c + 1) * cw)
+                part = project(cols)
+                part += jnp.dot(pick, resv[:, cols], preferred_element_type=f32)
+                acc[:, :, cols] = part.reshape(groups, cap, cw)
+
+    def z_copy(k, h):
+        return remote(send.at[h, k], own.at[h, k], zs.at[h, k], zr.at[h, k], to_plane(k))
+
+    def x_copy(k, h):
+        return remote(own.at[h, k], peer.at[h, k], xs.at[h, k], xr.at[h, k], x_mate)
+
+    def hid_copy(k):
+        return remote(hid_send.at[k], hid_recv.at[k], gs.at[k], gr.at[k], x_mate)
+
+    def back_copy(k, h):
+        return remote(comb.at[h, k], ret.at[h, k], bs.at[h, k], br.at[h, k], to_plane(k))
+
+    def travels(step, i, action):
+        if i % 2:
+            pl.when(step[i] != here)(action)
+        else:
+            action()
+
+    def emit(i, h):
+        k = emit_order[i]
+        with jax.named_scope("y%d_%d" % (i, h)):
+            y_copy(k, h).wait_recv()
         cols = slice(h * hw, (h + 1) * hw)
         piece = (acc[k, :, cols] + yrecv[h, k].astype(f32)).astype(bf)
         send[h, k] = piece
-        if k == here:
-            own[h, k] = piece
-            go(remote(send.at[h, k], peer.at[h, k], xs.at[h, k], xr.at[h, k], x_mate))
-        else:
-            go(remote(send.at[h, k], own.at[h, k], zs.at[h, k], zr.at[h, k], to_plane(k)))
-
-    def relay(k, h):
-        with jax.named_scope("z%d_%d" % (k, h)):
-            remote(send.at[h, k], own.at[h, k], zs.at[h, k], zr.at[h, k], x_mate).wait_recv()
-        go(remote(own.at[h, k], peer.at[h, k], xs.at[h, k], xr.at[h, k], x_mate))
-
-    def hidden_of(buf, k):
+        if i % 2:
+            @pl.when(k == here)
+            def _():
+                own[h, here] = piece
+        travels(emit_order, i, lambda: z_copy(k, h).start())
+
+    def relay(i, h):
+        k = serve_order[i]
+        with jax.named_scope("z%d_%d" % (i, h)):
+            travels(serve_order, i, lambda: z_copy(k, h).wait_recv())
+        go(x_copy(k, h))
+
+    def hidden_of(parts):
         squares = gate_act = up_act = 0.0
         for h in range(halves):
             span = slice(h * hw, (h + 1) * hw)
-            wide = buf[h, k].astype(f32)
+            wide = jnp.concatenate([buf[h, k] for buf, k in parts], axis=0).astype(f32)
             squares = squares + jnp.sum(wide * wide, axis=1, keepdims=True)
             block = (wide * gain_ref[:, span]).astype(bf)
             gate_act = gate_act + jnp.dot(block, gv[span, :], preferred_element_type=f32)
@@ -352,30 +384,36 @@
         g = gate_act * scale
         return (g / (1.0 + jnp.exp(-g)) * (up_act * scale)).astype(bf)
 
-    def expert_own(k):
-        with jax.named_scope("own%d" % k):
-            hid_own[k] = hidden_of(own, k)
-
-    def expert_peer(k):
-        with jax.named_scope("x%d" % k):
-            for h in range(halves):
-                remote(own.at[h, k], peer.at[h, k], xs.at[h, k], xr.at[h, k], x_mate).wait_recv()
-        with jax.named_scope("peer%d" % k):
-            hid_send[k] = hidden_of(peer, k)
-            go(remote(hid_send.at[k], hid_recv.at[k], gs.at[k], gr.at[k], x_mate))
+    def experts(i):
+        parts = []
+        if i < groups:
+            parts.append((own, serve_order[i]))
+        if i:
+            k = serve_order[i - 1]
+            with jax.named_scope("x%d" % i):
+                for h in range(halves):
+                    x_copy(k, h).wait_recv()
+            parts.append((peer, k))
+        with jax.named_scope("experts%d" % i):
+            result = hidden_of(parts)
+            if i:
+                hid_send[k] = result[-cap:]
+                go(hid_copy(k))
+            if i < groups:
+                hid_own[serve_order[i]] = result[:cap]
 
     sub_c = lax.broadcasted_iota(jnp.int32, (cap, rows), 0)
     lane_c = lax.broadcasted_iota(jnp.int32, (cap, rows), 1)
 
-    def combine(k):
-        with jax.named_scope("hid%d" % k):
-            remote(hid_send.at[k], hid_recv.at[k], gs.at[k], gr.at[k], x_mate).wait_recv()
-            if k == here:
-                table = wsend[...]
-            else:
-                remote(wsend, wrecv.at[k], ws.at[k], wr.at[k], x_mate).wait_recv()
-                table = wrecv[k]
-        with jax.named_scope("down%d" % k):
+    def combine(i):
+        k = serve_order[i]
+        with jax.named_scope("hid%d" % i):
+            hid_copy(k).wait_recv()
+            travels(serve_order, i, lambda: remote(
+                wsend, wrecv.at[k], ws.at[k], wr.at[k], x_mate
+            ).wait_recv())
+        with jax.named_scope("down%d" % i):
+            table = wrecv[k]
             chosen = lane_c == sub_c + k * cap
             w_own = jnp.sum(jnp.where(chosen, table[0:1, :], 0.0), axis=1, keepdims=True)
             w_peer = jnp.sum(jnp.where(chosen, table[1:2, :], 0.0), axis=1, keepdims=True)
@@ -386,52 +424,48 @@
                     total = jnp.dot(mine, dv[:, cols], preferred_element_type=f32) * w_own
                     total += jnp.dot(theirs, dv_mate[:, cols], preferred_element_type=f32) * w_peer
                     comb[h, k, :, c * cw:(c + 1) * cw] = total.astype(bf)
-                if k != here:
-                    go(remote(comb.at[h, k], ret.at[h, k], bs.at[h, k], br.at[h, k], to_plane(k)))
+                travels(serve_order, i, lambda h=h: back_copy(k, h).start())
 
     def finish(k, h):
         if k == here:
             back = comb[h, k]
         else:
             with jax.named_scope("r%d_%d" % (k, h)):
-                remote(comb.at[h, k], ret.at[h, k], bs.at[h, k], br.at[h, k], x_mate).wait_recv()
+                back_copy(k, h).wait_recv()
             back = ret[h, k]
         total = send[h, k].astype(f32) + back.astype(f32)
         fin[k * cap:(k + 1) * cap, h * hw:(h + 1) * hw] = total.astype(bf)
 
-    hs_all = range(halves)
-    for k in (0, here):
-        for h in hs_all:
-            emit(k, h)
+    gather_rows(pick, att[tp], am_near[...])
+    for h in range(halves):
+        near_project(h)
+        emit(0, h)
+    for i in (1, 2):
+        for h in range(halves):
+            emit(i, h)
+            relay(i - 1, h)
+        experts(i - 1)
+    for h in range(halves):
+        emit(3, h)
+        relay(2, h)
     with jax.named_scope("dmate"):
         d_copy.wait_recv()
     d_fwd = go(remote(
         dv_mate.at[own_half], dv_mate.at[own_half], ds.at[1], dr_sem.at[1], {"tp": mate}
     ))
-    expert_own(here)
-    for h in hs_all[:-1]:
-        relay(0, h)
-    for h in hs_all:
-        emit(2, h)
-    relay(0, halves - 1)
-    expert_own(0)
-    expert_peer(here)
-    for h in hs_all:
-        emit(3, h)
+    experts(2)
     d_fwd.wait_recv()
-    combine(here)
-    expert_peer(0)
+    for h in range(halves - 1):
+        relay(3, h)
     combine(0)
-    for k in (3, 2):
-        for h in hs_all:
-            relay(k, h)
-        expert_own(k)
-    for k in (3, 2):
-        expert_peer(k)
-    for k in (3, 2):
-        combine(k)
-    for k in (here, 0, 3, 2):
-        for h in hs_all:
+    relay(3, halves - 1)
+    experts(3)
+    combine(1)
+    experts(4)
+    combine(2)
+    combine(3)
+    for k in (0, 2, here, 1):
+        for h in range(halves):
             finish(k, h)
     with jax.named_scope("out"):
         spread_b = spread.astype(bf)
@@ -441,6 +475,10 @@
                 spread_b, fin[:, cols], preferred_element_type=f32
             ).astype(bf)
     with jax.named_scope("sends"):
+        for k in away:
+            for h in range(halves):
+                z_copy(k, h).wait_send()
+                back_copy(k, h).wait_send()
         for copy in pending:
             copy.wait_send()
 

time: 82.5 us -> 76.3 us (0.925)
  the two profiles are of different devices: /device:TPU:0 before, /device:TPU:8 now
where the time goes in v2:
time: 76.3 us; the launch traced here: 76 us
  Pallas kernels  73.7 us (97%)
  local copies, waits for them, and re-layouts  2.3 us (3%)
    pallas_call x1, Pallas kernels, mixture(): pl.pallas_call(functools.partial(moe_kernel, groups, HALVES), out_shape=j...  73.7 us
    unnamed x1, local copies, waits for them, and re-layouts  2.3 us

profile of v2, /device:TPU:8, one launch (start us, length us, event | category | flops | bytes accessed | tf_op | source)
XLA Modules:
  0.0 76.0 jit_solution(7999366669629889700)
XLA Ops:
  0.0 73.7 %mixture.1 = bf16[256,2048]{1,0:T(8,128)(2,1)} custom-call(f32[8]{0:T(128)} %sink_ref.1, s32[8,128]{1,0:T(8,128)} %bitcast.9, s32[2,256]{1,0:T(2,128)} %bitcast.10, f32[2,256]{1,0:T(2,128)} %bitcast.11, f32[1,2048]{1,0:T(1,128)} %bitcast.8, bf16[1024,512]{1,0:T(8,128)(2,1)} %q_hbm.1, bf16[8,128,128]{2,1,0:T(8,128)(2,1)} %bitcast.6, ...), custom_call_target="tpu_custom_call" | custom-call | tf_op jit(solution)/shard_map/mixture/pallas_call | solution.py:709
  73.7 2.3 %copy.15 = bf16[256,2048]{1,0:T(8,128)(2,1)} copy(bf16[256,2048]{1,0:T(8,128)(2,1)} %mixture.1) | data formatting | bytes 2097152

commit v3 on v2

--- a/solution.py
+++ b/solution.py
@@ -103,13 +103,14 @@
 
 def moe_kernel(
     groups, halves,
-    sink_ref, doc_ref, routes_ref, rw_ref, gain_ref,
+    sink_hbm, doc_hbm, routes_hbm, rw_hbm, gain_hbm,
     q_hbm, k_hbm, v_hbm, res_hbm, w_hbm, gate_hbm, up_hbm, down_hbm,
-    out_ref,
+    moved_hbm, spread_hbm,
+    fin, spread_ref, sink_ref, doc_ref, routes_ref, rw_ref, gain_ref,
     qv, resv, wv, w_mate, kx, vx, dl, dr, dx, att, am_far, am_near, routes_far,
     mixed_att, acc, ysend, yrecv, send, own, peer, comb, ret, hid_own, hid_send, hid_recv,
-    wsend, wrecv, fin, gv, uv, dv, dv_mate,
-    ls, hs, hr, ms, mr, ys, yr, zs, zr, xs, xr, gs, gr, bs, br, ws, wr, ds, dr_sem,
+    wsend, wrecv, gv, uv, dv, dv_mate,
+    ls, hs, hr, ms, mr, ys, yr, zs, zr, xs, xr, gs, gr, bs, br, ws, wr, ds, dr_sem, outs,
 ):
     sp = lax.axis_index("sp")
     tp = lax.axis_index("tp")
@@ -125,7 +126,7 @@
     order = plane_order(gz)
     here = groups - 1
     away = [k for k in range(groups) if k != here]
-    rows, width = out_ref.shape
+    rows, width = fin.shape
     cap = rows // groups
     hw = width // halves
     cw = width // 4
@@ -149,8 +150,8 @@
     def pick_one(at_end, at_middle):
         return at_end if at_end == at_middle else jnp.where(end, at_end, at_middle)
 
-    emit_order = [pick_one(a, b) for a, b in ((0, 2), (1, 3), (2, 0), (3, 1))]
-    serve_order = [pick_one(a, b) for a, b in ((2, 0), (1, 3), (0, 2), (3, 1))]
+    emit_order = [pick_one(a, b) for a, b in ((0, 2), (1, 0), (2, 1), (here, here))]
+    serve_order = [pick_one(a, b) for a, b in ((2, 0), (1, 2), (0, 1), (here, here))]
 
     def to_plane(k):
         plane = order[3]
@@ -163,18 +164,97 @@
     partners += [to_plane(k) for k in away]
     for where in partners:
         pl.semaphore_signal(barrier, inc=1, device_id=where, device_id_type=mesh_id)
-    loads = [
-        pltpu.make_async_copy(src, dst, ls.at[i])
-        for i, (src, dst) in enumerate((
-            (k_hbm, kx.at[pl.ds(1, blocks)]), (v_hbm, vx.at[pl.ds(1, blocks)]), (q_hbm, qv),
-            (w_hbm, wv), (res_hbm, resv), (gate_hbm.at[0], gv), (up_hbm.at[0], uv),
-            (down_hbm.at[0], dv),
-        ))
+    pairs = (
+        (k_hbm, kx.at[pl.ds(1, blocks)]), (v_hbm, vx.at[pl.ds(1, blocks)]),
+        (doc_hbm, doc_ref), (routes_hbm, routes_ref), (rw_hbm, rw_ref), (sink_hbm, sink_ref),
+        (q_hbm, qv), (w_hbm, wv), (gain_hbm, gain_ref), (res_hbm, resv),
+        (gate_hbm.at[0], gv), (up_hbm.at[0], uv), (down_hbm.at[0], dv),
+    )
+    loads = [pltpu.make_async_copy(src, dst, ls.at[i]) for i, (src, dst) in enumerate(pairs)]
+    for load in loads[:7]:
+        load.start()
+
+    @pl.when(sp == 0)
+    def _():
+        kx[0] = jnp.zeros(kx.shape[1:], bf)
+        vx[0] = jnp.zeros(vx.shape[1:], bf)
+
+    @pl.when(sp == sp_count - 1)
+    def _():
+        kx[blocks + 1] = jnp.zeros(kx.shape[1:], bf)
+        vx[blocks + 1] = jnp.zeros(vx.shape[1:], bf)
+
+    for load in loads[:5]:
+        load.wait()
+    with jax.named_scope("barrier"):
+        pl.semaphore_wait(barrier, len(partners))
+    pending = []
+
+    def go(copy):
+        copy.start()
+        pending.append(copy)
+        return copy
+
+    def halo_of(i, src, dst, where):
+        return remote(src, dst, hs.at[i], hr.at[i], {"sp": where})
+
+    to_after = [
+        halo_of(0, kx.at[blocks], kx.at[0], after),
+        halo_of(1, vx.at[blocks], vx.at[0], after),
+        halo_of(2, doc_ref, dl, after),
     ]
-    for load in loads:
-        load.start()
+    to_before = [
+        halo_of(3, kx.at[1], kx.at[blocks + 1], before),
+        halo_of(4, vx.at[1], vx.at[blocks + 1], before),
+        halo_of(5, doc_ref, dr, before),
+    ]
+
+    @pl.when(sp > 0)
+    def _():
+        for copy in to_before:
+            copy.start()
+
+    @pl.when(sp < sp_count - 1)
+    def _():
+        for copy in to_after:
+            copy.start()
+
+    r_copy = go(remote(routes_ref, routes_far, ms.at[3], mr.at[3], {"tp": across}))
+    ff = dv.shape[0]
+    quarter, eighth = ff // 4, ff // 8
+    chip = tp // 2
+    d_rows = [
+        pl.ds(pl.multiple_of(start, eighth), count) for start, count in (
+            ((2 + chip) * quarter + core * eighth, eighth), (core * quarter, quarter),
+            ((3 - chip) * quarter + core * eighth, eighth),
+        )
+    ]
+
+    def d_part(i, source, sem, where):
+        return remote(
+            source.at[d_rows[i]], dv_mate.at[d_rows[i]], ds.at[sem], dr_sem.at[sem], where
+        )
+
+    from_x = [go(d_part(i, down_hbm.at[0], i, x_mate)) for i in range(2)]
+    w_copy = remote(w_hbm, w_mate, ms.at[0], mr.at[0], {"tp": mate})
     for b in range(blocks):
         dx[b + 1] = jnp.broadcast_to(doc_ref[b:b + 1, :].astype(f32), (8, WINDOW))
+
+    def left_halo():
+        @pl.when(sp > 0)
+        def _():
+            for copy in to_after:
+                copy.wait_recv()
+        left = jnp.where(sp == 0, -1.0, dl[blocks - 1:blocks, :].astype(f32))
+        dx[0] = jnp.broadcast_to(left, (8, WINDOW))
+
+    def right_halo():
+        @pl.when(sp < sp_count - 1)
+        def _():
+            for copy in to_before:
+                copy.wait_recv()
+        right = jnp.where(sp == sp_count - 1, -1.0, dr[0:1, :].astype(f32))
+        dx[blocks + 1] = jnp.broadcast_to(right, (8, WINDOW))
 
     slot = slots_of(routes_ref[...], order, cap)
     ri = lax.broadcasted_iota(jnp.int32, (rows, rows), 0)
@@ -193,32 +273,8 @@
 
     wrecv[here] = wsend[...]
 
-    loads[0].wait()
-    loads[1].wait()
-    pl.semaphore_wait(barrier, len(partners))
-    pending = []
-
-    def go(copy):
-        copy.start()
-        pending.append(copy)
-        return copy
-
-    halo = [
-        go(remote(src, dst, hs.at[i], hr.at[i], {"sp": where}))
-        for i, (src, dst, where) in enumerate((
-            (kx.at[blocks], kx.at[0], after), (vx.at[blocks], vx.at[0], after),
-            (doc_ref, dl, after),
-            (kx.at[1], kx.at[blocks + 1], before), (vx.at[1], vx.at[blocks + 1], before),
-            (doc_ref, dr, before),
-        ))
-    ]
-    w_copy = go(remote(w_hbm, w_mate, ms.at[0], mr.at[0], {"tp": mate}))
-    r_copy = go(remote(routes_ref, routes_far, ms.at[3], mr.at[3], {"tp": across}))
     for k in away:
         go(remote(wsend, wrecv.at[k], ws.at[k], wr.at[k], to_plane(k)))
-    ff = dv.shape[0]
-    own_half = pl.ds(core * (ff // 2), ff // 2)
-    d_copy = go(remote(down_hbm.at[0, own_half], dv_mate.at[own_half], ds.at[0], dr_sem.at[0], x_mate))
 
     qi = lax.broadcasted_iota(jnp.int32, (WINDOW, 3 * WINDOW), 0)
     ki = lax.broadcasted_iota(jnp.int32, (WINDOW, 3 * WINDOW), 1)
@@ -226,6 +282,10 @@
     eye = lax.broadcasted_iota(jnp.int32, (WINDOW, WINDOW), 0) == lax.broadcasted_iota(
         jnp.int32, (WINDOW, WINDOW), 1
     )
+
+    low = lax.broadcasted_iota(jnp.int32, (3 * WINDOW, kv_heads * HD), 1) < HD
+    low_q = lax.broadcasted_iota(jnp.int32, (WINDOW, kv_heads * HD), 1) < HD
+    zero, one = jnp.zeros((), bf), jnp.ones((), bf)
 
     def attend_block(b):
         own_docs = dx[b + 1][0:1]
@@ -234,40 +294,50 @@
         bias = jnp.where(band & (key_docs == query_docs), 0.0, neg_fill)
         keys = kx[pl.ds(b, 3)].reshape(3 * WINDOW, kv_heads * HD)
         values = vx[pl.ds(b, 3)].reshape(3 * WINDOW, kv_heads * HD)
+        key_two = jnp.concatenate(
+            [jnp.where(low, keys, zero), jnp.where(low, zero, keys)], axis=0
+        )
+        value_two = jnp.concatenate([
+            jnp.concatenate([jnp.where(low, values, zero), jnp.where(low, one, zero)], axis=1),
+            jnp.concatenate([jnp.where(low, zero, values), jnp.where(low, zero, one)], axis=1),
+        ], axis=0)
         home = b // home_blocks
         to_rows = pl.ds(pl.multiple_of((b % home_blocks) * WINDOW, WINDOW), WINDOW)
         from_rows = pl.ds(pl.multiple_of(b * WINDOW, WINDOW), WINDOW)
-        for g in range(kv_heads):
-            span = slice(g * ratio * HD, (g + 1) * ratio * HD)
-            q = qv[from_rows, span] * jnp.asarray(HD ** (-0.5), bf)
-            stacked = jnp.concatenate([q[:, r * HD:(r + 1) * HD] for r in range(ratio)], axis=0)
+        q = qv[from_rows, :] * jnp.asarray(HD ** (-0.5), bf)
+        parts = [None] * (2 * ratio)
+        for r in range(ratio):
+            pair = jnp.concatenate(
+                [q[:, r * HD:(r + 1) * HD], q[:, (ratio + r) * HD:(ratio + r + 1) * HD]], axis=1
+            )
             scores = lax.dot_general(
-                stacked, keys[:, g * HD:(g + 1) * HD], (((1,), (1,)), ((), ())),
-                preferred_element_type=f32,
+                pair, key_two, (((1,), (1,)), ((), ())), preferred_element_type=f32
             )
-            vg = values[:, g * HD:(g + 1) * HD]
-            parts = []
-            for r in range(ratio):
+            exps, sinks = [], []
+            for g in range(2):
                 sink = sink_ref[g * ratio + r]
-                s = scores[r * WINDOW:(r + 1) * WINDOW] + bias
+                s = scores[:, g * 3 * WINDOW:(g + 1) * 3 * WINDOW] + bias
                 top = jnp.maximum(jnp.max(s, axis=1, keepdims=True), sink)
-                e = jnp.exp(s - top)
-                den = jnp.sum(e, axis=1, keepdims=True) + jnp.exp(sink - top)
-                o = jnp.dot(e.astype(bf), vg, preferred_element_type=f32)
-                parts.append((o / den).astype(bf))
-            att[home, to_rows, span] = jnp.concatenate(parts, axis=1)
+                exps.append(jnp.exp(s - top).astype(bf))
+                sinks.append(jnp.exp(sink - top))
+            o = jnp.dot(jnp.concatenate(exps, axis=1), value_two, preferred_element_type=f32)
+            den = o[:, 2 * HD:] + jnp.where(low_q, sinks[0], sinks[1])
+            both = (o[:, :2 * HD] / den).astype(bf)
+            parts[r], parts[ratio + r] = both[:, :HD], both[:, HD:]
+        att[home, to_rows, :] = jnp.concatenate(parts, axis=1)
 
     def far_step(i, carry):
-        @pl.when(i == half - 1)
+        @pl.when(i == 1)
         def _():
-            for copy in halo:
-                copy.wait_recv()
-            left = dl[blocks - 1:blocks, :].astype(f32)
-            right = dr[0:1, :].astype(f32)
-            left = jnp.where(sp == 0, -1.0, left)
-            right = jnp.where(sp == sp_count - 1, -1.0, right)
-            dx[0] = jnp.broadcast_to(left, (8, WINDOW))
-            dx[blocks + 1] = jnp.broadcast_to(right, (8, WINDOW))
+            w_copy.start()
+
+        @pl.when((i == half - 1) & (tp < 2))
+        def _():
+            right_halo()
+
+        @pl.when((i == half - 1) & (tp >= 2))
+        def _():
+            left_halo()
 
         attend_block(jnp.where(tp < 2, half + i, half - 1 - i))
         return carry
@@ -283,14 +353,28 @@
         part = jnp.dot(mixed_att[:, :heads], wv[:, cols], preferred_element_type=f32)
         return part + jnp.dot(mixed_att[:, heads:], w_mate[:, cols], preferred_element_type=f32)
 
-    loads[2].wait()
+    def near_step(i, carry):
+        own_turn = tp * home_blocks + i - home_blocks
+        attend_block(jnp.where(i < home_blocks, mate * home_blocks + i, own_turn))
+        return carry
+
+    loads[5].wait()
+    loads[6].wait()
+    loads[7].start()
     with jax.named_scope("attn_far"):
         lax.fori_loop(0, half, far_step, 0)
+    pending.append(w_copy)
     far_copy = go(remote(att.at[mate_across], am_far, ms.at[1], mr.at[1], {"tp": mate}))
+    for load in loads[8:]:
+        load.start()
+    with jax.named_scope("attn_first"):
+        pl.when(tp < 2)(left_halo)
+        pl.when(tp >= 2)(right_halo)
+        near_step(0, 0)
     with jax.named_scope("wait_far"):
         r_copy.wait_recv()
         pick_far = pick_of(slots_of(routes_far[...], order, cap))
-        loads[3].wait()
+        loads[7].wait()
         w_copy.wait_recv()
         far_copy.wait_recv()
     with jax.named_scope("far_proj"):
@@ -310,19 +394,20 @@
             if h < halves - 1:
                 go(y_copy(emit_order[0], h))
         go(y_copy(emit_order[0], halves - 1))
-        for k in emit_order[1:]:
+        for k in emit_order[1:here]:
             for h in range(halves):
                 go(y_copy(k, h))
 
-    def near_step(i, carry):
-        attend_block(jnp.where(tp < 2, half - 1 - i, half + i))
-        return carry
-
     with jax.named_scope("attn_near"):
-        lax.fori_loop(0, half, near_step, 0)
-    near_copy = go(remote(att.at[mate], am_near, ms.at[2], mr.at[2], {"tp": mate}))
-    for i in range(4, 8):
-        loads[i].wait()
+        lax.fori_loop(1, home_blocks, near_step, 0)
+        near_copy = go(remote(att.at[mate], am_near, ms.at[2], mr.at[2], {"tp": mate}))
+        from_x[0].wait_recv()
+        go(d_part(0, dv_mate, 2, {"tp": across}))
+        for h in range(halves):
+            go(y_copy(here, h))
+        lax.fori_loop(home_blocks, half, near_step, 0)
+    for load in loads[8:]:
+        load.wait()
     with jax.named_scope("wait_near"):
         pick = pick_of(slot)
         near_copy.wait_recv()
@@ -346,12 +431,6 @@
     def back_copy(k, h):
         return remote(comb.at[h, k], ret.at[h, k], bs.at[h, k], br.at[h, k], to_plane(k))
 
-    def travels(step, i, action):
-        if i % 2:
-            pl.when(step[i] != here)(action)
-        else:
-            action()
-
     def emit(i, h):
         k = emit_order[i]
         with jax.named_scope("y%d_%d" % (i, h)):
@@ -359,16 +438,16 @@
         cols = slice(h * hw, (h + 1) * hw)
         piece = (acc[k, :, cols] + yrecv[h, k].astype(f32)).astype(bf)
         send[h, k] = piece
-        if i % 2:
-            @pl.when(k == here)
-            def _():
-                own[h, here] = piece
-        travels(emit_order, i, lambda: z_copy(k, h).start())
+        if i == here:
+            own[h, here] = piece
+        else:
+            z_copy(k, h).start()
 
     def relay(i, h):
         k = serve_order[i]
-        with jax.named_scope("z%d_%d" % (i, h)):
-            travels(serve_order, i, lambda: z_copy(k, h).wait_recv())
+        if i != here:
+            with jax.named_scope("z%d_%d" % (i, h)):
+                z_copy(k, h).wait_recv()
         go(x_copy(k, h))
 
     def hidden_of(parts):
@@ -409,9 +488,8 @@
         k = serve_order[i]
         with jax.named_scope("hid%d" % i):
             hid_copy(k).wait_recv()
-            travels(serve_order, i, lambda: remote(
-                wsend, wrecv.at[k], ws.at[k], wr.at[k], x_mate
-            ).wait_recv())
+            if i != here:
+                remote(wsend, wrecv.at[k], ws.at[k], wr.at[k], x_mate).wait_recv()
         with jax.named_scope("down%d" % i):
             table = wrecv[k]
             chosen = lane_c == sub_c + k * cap
@@ -424,7 +502,8 @@
                     total = jnp.dot(mine, dv[:, cols], preferred_element_type=f32) * w_own
                     total += jnp.dot(theirs, dv_mate[:, cols], preferred_element_type=f32) * w_peer
                     comb[h, k, :, c * cw:(c + 1) * cw] = total.astype(bf)
-                travels(serve_order, i, lambda h=h: back_copy(k, h).start())
+                if i != here:
+                    back_copy(k, h).start()
 
     def finish(k, h):
         if k == here:
@@ -434,53 +513,98 @@
                 back_copy(k, h).wait_recv()
             back = ret[h, k]
         total = send[h, k].astype(f32) + back.astype(f32)
-        fin[k * cap:(k + 1) * cap, h * hw:(h + 1) * hw] = total.astype(bf)
-
+        block = (slice(k * cap, (k + 1) * cap), slice(h * hw, (h + 1) * hw))
+        fin[block] = total.astype(bf)
+        store = pltpu.make_async_copy(fin.at[block], moved_hbm.at[block], outs.at[k * halves + h])
+        store.start()
+        stores.append(store)
+
+    spread_ref[...] = spread.astype(bf)
+    stores = [pltpu.make_async_copy(spread_ref, spread_hbm, outs.at[groups * halves])]
+    stores[0].start()
     gather_rows(pick, att[tp], am_near[...])
     for h in range(halves):
         near_project(h)
         emit(0, h)
-    for i in (1, 2):
-        for h in range(halves):
-            emit(i, h)
-            relay(i - 1, h)
-        experts(i - 1)
     for h in range(halves):
-        emit(3, h)
+        emit(1, h)
+        relay(0, h)
+    from_x[1].wait_recv()
+    to_mate = [go(d_part(j, dv_mate, 3 + j, {"tp": mate})) for j in range(2)]
+    experts(0)
+    for h in range(halves):
+        emit(2, h)
+        relay(1, h)
+    experts(1)
+    for h in range(halves - 1):
         relay(2, h)
     with jax.named_scope("dmate"):
-        d_copy.wait_recv()
-    d_fwd = go(remote(
-        dv_mate.at[own_half], dv_mate.at[own_half], ds.at[1], dr_sem.at[1], {"tp": mate}
-    ))
+        d_part(2, dv_mate, 2, {"tp": across}).wait_recv()
+        to_mate.append(go(d_part(2, dv_mate, 5, {"tp": mate})))
+    emit(here, 0)
+    for copy in to_mate:
+        copy.wait_recv()
+    combine(0)
+    relay(2, halves - 1)
     experts(2)
-    d_fwd.wait_recv()
-    for h in range(halves - 1):
-        relay(3, h)
-    combine(0)
-    relay(3, halves - 1)
+    for h in range(1, halves):
+        emit(here, h)
+    for h in range(halves):
+        relay(here, h)
+    combine(1)
     experts(3)
-    combine(1)
+    combine(2)
     experts(4)
-    combine(2)
-    combine(3)
+    combine(here)
     for k in (0, 2, here, 1):
         for h in range(halves):
             finish(k, h)
-    with jax.named_scope("out"):
-        spread_b = spread.astype(bf)
-        for c in range(4):
-            cols = slice(c * cw, (c + 1) * cw)
-            out_ref[:, cols] = jnp.dot(
-                spread_b, fin[:, cols], preferred_element_type=f32
-            ).astype(bf)
+    for store in stores:
+        store.wait()
     with jax.named_scope("sends"):
         for k in away:
             for h in range(halves):
                 z_copy(k, h).wait_send()
                 back_copy(k, h).wait_send()
+        @pl.when(sp > 0)
+        def _():
+            for copy in to_before:
+                copy.wait_send()
+
+        @pl.when(sp < sp_count - 1)
+        def _():
+            for copy in to_after:
+                copy.wait_send()
+
         for copy in pending:
             copy.wait_send()
+
+
+def place_kernel(spread_hbm, rows_hbm, out_hbm, spread, moved, out, ls, ss):
+    parts = ls.shape[0] - 1
+    cw = out.shape[1] // parts
+    cols = [slice(c * cw, (c + 1) * cw) for c in range(parts)]
+    first = pltpu.make_async_copy(spread_hbm, spread, ls.at[parts])
+    first.start()
+    loads = [
+        pltpu.make_async_copy(rows_hbm.at[:, c], moved.at[:, c], ls.at[i])
+        for i, c in enumerate(cols)
+    ]
+    stores = [
+        pltpu.make_async_copy(out.at[:, c], out_hbm.at[:, c], ss.at[i])
+        for i, c in enumerate(cols)
+    ]
+    for load in loads:
+        load.start()
+    first.wait()
+    for c, load, store in zip(cols, loads, stores):
+        load.wait()
+        out[:, c] = jnp.dot(
+            spread[...], moved[:, c], preferred_element_type=jnp.float32
+        ).astype(out.dtype)
+        store.start()
+    for store in stores:
+        store.wait()
 
 
 def front_kernel(
@@ -702,16 +826,21 @@
     pieces = pltpu.VMEM((HALVES, groups, cap, hw), bf)
     hidden = pltpu.VMEM((groups, cap, ff), bf)
     dma = pltpu.SemaphoreType.DMA
-    vm = pl.BlockSpec(memory_space=pltpu.VMEM)
     hbm = pl.BlockSpec(memory_space=pl.ANY)
     edge = pltpu.VMEM((blocks + 2, WINDOW, kv_width), bf)
     per_piece = dma((HALVES, groups))
-    return pl.pallas_call(
+    moved, spread = pl.pallas_call(
         functools.partial(moe_kernel, groups, HALVES),
-        out_shape=jax.ShapeDtypeStruct((rows, width), bf),
-        in_specs=[pl.BlockSpec(memory_space=pltpu.SMEM)] + [vm] * 4 + [hbm] * 8,
-        out_specs=vm,
+        out_shape=(
+            jax.ShapeDtypeStruct((rows, width), bf), jax.ShapeDtypeStruct((rows, rows), bf)
+        ),
+        in_specs=[hbm] * 13,
+        out_specs=(hbm, hbm),
         scratch_shapes=[
+            pltpu.VMEM((rows, width), bf), pltpu.VMEM((rows, rows), bf),
+            pltpu.SMEM(sink_logit.shape, f32), pltpu.VMEM(docs.shape, i32),
+            pltpu.VMEM(routes.shape[::-1], i32), pltpu.VMEM(routes.shape[::-1], f32),
+            pltpu.VMEM((1, width), f32),
             pltpu.VMEM(queries.shape, bf), pltpu.VMEM((rows, width), bf),
             pltpu.VMEM(out_weight.shape, bf), pltpu.VMEM(out_weight.shape, bf),
             edge, edge,
@@ -725,13 +854,13 @@
             pieces, pieces, pieces, pieces, pieces, pieces, pieces,
             hidden, hidden, hidden,
             pltpu.VMEM((8, rows), f32), pltpu.VMEM((groups, 8, rows), f32),
-            pltpu.VMEM((rows, width), bf),
             pltpu.VMEM((width, ff), bf), pltpu.VMEM((width, ff), bf),
             pltpu.VMEM((ff, width), bf), pltpu.VMEM((ff, width), bf),
-            dma((8,)), dma((6,)), dma((6,)), dma((4,)), dma((4,)),
+            dma((13,)), dma((6,)), dma((6,)), dma((4,)), dma((4,)),
             per_piece, per_piece, per_piece, per_piece, per_piece, per_piece,
             dma((groups,)), dma((groups,)), per_piece, per_piece,
-            dma((groups,)), dma((groups,)), dma((2,)), dma((2,)),
+            dma((groups,)), dma((groups,)), dma((6,)), dma((6,)),
+            dma((groups * HALVES + 1,)),
         ],
         compiler_params=pltpu.CompilerParams(
             collective_id=3, has_side_effects=True, vmem_limit_bytes=56 * 1024 * 1024
@@ -743,6 +872,17 @@
         value_rows.reshape(blocks, WINDOW, kv_width), residual, out_weight,
         gate_weight, up_weight, down_weight,
     )
+    return pl.pallas_call(
+        place_kernel,
+        out_shape=jax.ShapeDtypeStruct((rows, width), bf),
+        in_specs=[hbm, hbm],
+        out_specs=hbm,
+        scratch_shapes=[
+            pltpu.VMEM((rows, rows), bf), pltpu.VMEM((rows, width), bf),
+            pltpu.VMEM((rows, width), bf), dma((5,)), dma((4,)),
+        ],
+        name="place",
+    )(spread, moved)
 
 
 def fits_front(queries):

time: 76.3 us -> 70.3 us (0.921)
  Pallas kernels: 73.7 us -> 69.3 us
  local copies, waits for them, and re-layouts: 2.3 us -> 0 us
    pallas_call x1 -> x2, Pallas kernels: 73.7 us -> 69.3 us  [the longest x1 66.5 us: mixture(): pl.pallas_call(functools.partial(moe_kernel, groups, HALVES), out_shape=(...]
    unnamed x1 -> x0, local copies, waits for them, and re-layouts: 2.3 us -> none
where the time goes in v3:
time: 70.3 us; the launch traced here: 69.3 us
  Pallas kernels  69.3 us (99%)
    pallas_call x1, Pallas kernels, mixture(): pl.pallas_call(functools.partial(moe_kernel, groups, HALVES), out_shape=(...  66.5 us
    pallas_call x1, Pallas kernels, mixture(): pl.pallas_call(place_kernel, out_shape=jax.ShapeDtypeStruct((rows, width)...  2.74 us

profile of v3, /device:TPU:8, one launch (start us, length us, event | category | flops | bytes accessed | tf_op | source)
XLA Modules:
  0.0 69.3 jit_solution(5934943765812894437)
XLA Ops:
  0.0 66.5 %mixture.1 = (bf16[256,2048]{1,0:T(8,128)(2,1)}, bf16[256,256]{1,0:T(8,128)(2,1)}) custom-call(f32[8]{0:T(128)} %sink_hbm.1, s32[8,128]{1,0:T(8,128)} %bitcast.9, s32[2,256]{1,0:T(2,128)} %bitcast.10, f32[2,256]{1,0:T(2,128)} %bitcast.11, f32[1,2048]{1,0:T(1,128)} %bitcast.8, bf16[1024,512]{1,0:T(8,128)(2,1)} %q_hbm.1, bf16[8,128,128]{2,1,0:T(8,128)(2,1)} %bitcast.6, ...), custom_call_target="tpu_custom_call" | custom-call | tf_op jit(solution)/shard_map/mixture/pallas_call | solution.py:832
  66.5 2.7 %place.1 = bf16[256,2048]{1,0:T(8,128)(2,1)} custom-call(bf16[256,256]{1,0:T(8,128)(2,1)} %get-tuple-element.7.spread_hbm, bf16[256,2048]{1,0:T(8,128)(2,1)} %get-tuple-element.8.rows_hbm), custom_call_target="tpu_custom_call" | custom-call | tf_op jit(solution)/shard_map/place/pallas_call | solution.py:875

commit v4 on v3

--- a/solution.py
+++ b/solution.py
@@ -150,8 +150,8 @@
     def pick_one(at_end, at_middle):
         return at_end if at_end == at_middle else jnp.where(end, at_end, at_middle)
 
-    emit_order = [pick_one(a, b) for a, b in ((0, 2), (1, 0), (2, 1), (here, here))]
-    serve_order = [pick_one(a, b) for a, b in ((2, 0), (1, 2), (0, 1), (here, here))]
+    emit_order = [pick_one(a, b) for a, b in ((1, 2), (0, 0), (2, 1), (here, here))]
+    serve_order = [pick_one(a, b) for a, b in ((1, 0), (2, 2), (0, 1), (here, here))]
 
     def to_plane(k):
         plane = order[3]
@@ -209,16 +209,20 @@
         halo_of(5, doc_ref, dr, before),
     ]
 
-    @pl.when(sp > 0)
-    def _():
-        for copy in to_before:
-            copy.start()
-
-    @pl.when(sp < sp_count - 1)
-    def _():
-        for copy in to_after:
-            copy.start()
-
+    def send_before():
+        @pl.when(sp > 0)
+        def _():
+            for copy in to_before:
+                copy.start()
+
+    def send_after():
+        @pl.when(sp < sp_count - 1)
+        def _():
+            for copy in to_after:
+                copy.start()
+
+    pl.when(tp < 2)(send_before)
+    pl.when(tp >= 2)(send_after)
     r_copy = go(remote(routes_ref, routes_far, ms.at[3], mr.at[3], {"tp": across}))
     ff = dv.shape[0]
     quarter, eighth = ff // 4, ff // 8
@@ -235,7 +239,7 @@
             source.at[d_rows[i]], dv_mate.at[d_rows[i]], ds.at[sem], dr_sem.at[sem], where
         )
 
-    from_x = [go(d_part(i, down_hbm.at[0], i, x_mate)) for i in range(2)]
+    from_x = [d_part(i, down_hbm.at[0], i, x_mate) for i in range(2)]
     w_copy = remote(w_hbm, w_mate, ms.at[0], mr.at[0], {"tp": mate})
     for b in range(blocks):
         dx[b + 1] = jnp.broadcast_to(doc_ref[b:b + 1, :].astype(f32), (8, WINDOW))
@@ -326,71 +330,114 @@
             parts[r], parts[ratio + r] = both[:, :HD], both[:, HD:]
         att[home, to_rows, :] = jnp.concatenate(parts, axis=1)
 
-    def far_step(i, carry):
+    early = (tp == 1) | (tp == 2)
+    far_copy = remote(att.at[mate_across], am_far, ms.at[1], mr.at[1], {"tp": mate})
+    near_copy = remote(att.at[mate], am_near, ms.at[2], mr.at[2], {"tp": mate})
+
+    low_side = tp < 2
+    starts = [
+        jnp.where(low_side, half, home_blocks), jnp.where(low_side, home_blocks, half),
+        jnp.where(low_side, half + home_blocks, 0), jnp.where(low_side, 0, half + home_blocks),
+    ]
+
+    def attend_home(start):
+        for j in range(home_blocks):
+            attend_block(start + j)
+
+    def first_pairs(i, carry):
+        @pl.when(i == 0)
+        def _():
+            w_copy.start()
+
+        @pl.when((i == 1) & early)
+        def _():
+            far_copy.start()
+
+        @pl.when((i == 1) & low_side)
+        def _():
+            send_after()
+
+        @pl.when((i == 1) & jnp.logical_not(low_side))
+        def _():
+            send_before()
+
         @pl.when(i == 1)
         def _():
-            w_copy.start()
-
-        @pl.when((i == half - 1) & (tp < 2))
-        def _():
-            right_halo()
-
-        @pl.when((i == half - 1) & (tp >= 2))
-        def _():
-            left_halo()
-
-        attend_block(jnp.where(tp < 2, half + i, half - 1 - i))
+            for copy in from_x:
+                copy.start()
+
+        @pl.when((i == 2) & jnp.logical_not(early))
+        def _():
+            near_copy.start()
+
+        @pl.when((i == 2) & low_side)
+        def _():
+            with jax.named_scope("halo_right"):
+                right_halo()
+
+        @pl.when((i == 2) & jnp.logical_not(low_side))
+        def _():
+            with jax.named_scope("halo_left"):
+                left_halo()
+
+        attend_home(jnp.where(i == 0, starts[0], jnp.where(i == 1, starts[1], starts[2])))
         return carry
 
     def pick_of(slot_row):
         return jnp.where(ri.astype(f32) == slot_row, 1.0, 0.0).astype(bf)
 
-    def gather_rows(pick, mine, mates):
-        mixed_att[:, :heads] = jnp.dot(pick, mine, preferred_element_type=f32).astype(bf)
-        mixed_att[:, heads:] = jnp.dot(pick, mates, preferred_element_type=f32).astype(bf)
+    def gather_mine(pick, rows_in):
+        mixed_att[:, :heads] = jnp.dot(pick, rows_in, preferred_element_type=f32).astype(bf)
+
+    def gather_mates(pick, rows_in):
+        mixed_att[:, heads:] = jnp.dot(pick, rows_in, preferred_element_type=f32).astype(bf)
+
+    def project_mine(cols):
+        return jnp.dot(mixed_att[:, :heads], wv[:, cols], preferred_element_type=f32)
+
+    def project_mates(cols):
+        return jnp.dot(mixed_att[:, heads:], w_mate[:, cols], preferred_element_type=f32)
 
     def project(cols):
-        part = jnp.dot(mixed_att[:, :heads], wv[:, cols], preferred_element_type=f32)
-        return part + jnp.dot(mixed_att[:, heads:], w_mate[:, cols], preferred_element_type=f32)
-
-    def near_step(i, carry):
-        own_turn = tp * home_blocks + i - home_blocks
-        attend_block(jnp.where(i < home_blocks, mate * home_blocks + i, own_turn))
-        return carry
+        return project_mine(cols) + project_mates(cols)
 
     loads[5].wait()
     loads[6].wait()
     loads[7].start()
     with jax.named_scope("attn_far"):
-        lax.fori_loop(0, half, far_step, 0)
-    pending.append(w_copy)
-    far_copy = go(remote(att.at[mate_across], am_far, ms.at[1], mr.at[1], {"tp": mate}))
+        lax.fori_loop(0, 3, first_pairs, 0)
+    pl.when(jnp.logical_not(early))(far_copy.start)
+    pending += [w_copy, far_copy, near_copy] + from_x
     for load in loads[8:]:
         load.start()
-    with jax.named_scope("attn_first"):
-        pl.when(tp < 2)(left_halo)
-        pl.when(tp >= 2)(right_halo)
-        near_step(0, 0)
-    with jax.named_scope("wait_far"):
+    per = 4 // halves
+    with jax.named_scope("far_mine"):
         r_copy.wait_recv()
         pick_far = pick_of(slots_of(routes_far[...], order, cap))
+        gather_mine(pick_far, att[across])
         loads[7].wait()
+        for c in range(per):
+            cols = slice(c * cw, (c + 1) * cw)
+            acc[:, :, cols] = project_mine(cols).reshape(groups, cap, cw)
+    with jax.named_scope("wait_far"):
         w_copy.wait_recv()
         far_copy.wait_recv()
     with jax.named_scope("far_proj"):
-        gather_rows(pick_far, att[across], am_far[...])
+        gather_mates(pick_far, am_far[...])
 
         def y_copy(k, h):
             return remote(
                 ysend.at[h, k], yrecv.at[h, k], ys.at[h, k], yr.at[h, k], {"tp": across}
             )
 
-        per = 4 // halves
         for h in range(halves):
             for c in range(per):
                 cols = slice(h * hw + c * cw, h * hw + (c + 1) * cw)
-                part = project(cols).astype(bf).reshape(groups, cap, cw)
-                ysend[h, :, :, c * cw:(c + 1) * cw] = part
+                if h:
+                    part = project(cols).reshape(groups, cap, cw)
+                else:
+                    part = project_mates(cols).reshape(groups, cap, cw) + acc[:, :, cols]
+                ysend[h, :, :, c * cw:(c + 1) * cw] = part.astype(bf)
             if h < halves - 1:
                 go(y_copy(emit_order[0], h))
         go(y_copy(emit_order[0], halves - 1))
@@ -399,25 +446,32 @@
                 go(y_copy(k, h))
 
     with jax.named_scope("attn_near"):
-        lax.fori_loop(1, home_blocks, near_step, 0)
-        near_copy = go(remote(att.at[mate], am_near, ms.at[2], mr.at[2], {"tp": mate}))
-        from_x[0].wait_recv()
-        go(d_part(0, dv_mate, 2, {"tp": across}))
-        for h in range(halves):
-            go(y_copy(here, h))
-        lax.fori_loop(home_blocks, half, near_step, 0)
+        pl.when(tp < 2)(left_halo)
+        pl.when(tp >= 2)(right_halo)
+        attend_home(starts[3])
+        pl.when(early)(near_copy.start)
     for load in loads[8:]:
         load.wait()
+    pick = pick_of(slot)
+    spread_ref[...] = spread.astype(bf)
+    stores = [pltpu.make_async_copy(spread_ref, spread_hbm, outs.at[groups * halves])]
+    stores[0].start()
+    with jax.named_scope("near_mine"):
+        gather_mine(pick, att[tp])
+        for c in range(4):
+            cols = slice(c * cw, (c + 1) * cw)
+            part = project_mine(cols)
+            part += jnp.dot(pick, resv[:, cols], preferred_element_type=f32)
+            acc[:, :, cols] = part.reshape(groups, cap, cw)
     with jax.named_scope("wait_near"):
-        pick = pick_of(slot)
         near_copy.wait_recv()
+    gather_mates(pick, am_near[...])
+
     def near_project(h):
         with jax.named_scope("near_proj%d" % h):
             for c in range(per):
                 cols = slice(h * hw + c * cw, h * hw + (c + 1) * cw)
-                part = project(cols)
-                part += jnp.dot(pick, resv[:, cols], preferred_element_type=f32)
-                acc[:, :, cols] = part.reshape(groups, cap, cw)
+                acc[:, :, cols] += project_mates(cols).reshape(groups, cap, cw)
 
     def z_copy(k, h):
         return remote(send.at[h, k], own.at[h, k], zs.at[h, k], zr.at[h, k], to_plane(k))
@@ -449,6 +503,16 @@
             with jax.named_scope("z%d_%d" % (i, h)):
                 z_copy(k, h).wait_recv()
         go(x_copy(k, h))
+
+    def relay_when(here_now, i, h):
+        k = serve_order[i]
+
+        @pl.when(here_now)
+        def _():
+            z_copy(k, h).wait_recv()
+            x_copy(k, h).start()
+
+        return x_copy(k, h)
 
     def hidden_of(parts):
         squares = gate_act = up_act = 0.0
@@ -464,22 +528,15 @@
         return (g / (1.0 + jnp.exp(-g)) * (up_act * scale)).astype(bf)
 
     def experts(i):
-        parts = []
-        if i < groups:
-            parts.append((own, serve_order[i]))
-        if i:
-            k = serve_order[i - 1]
-            with jax.named_scope("x%d" % i):
-                for h in range(halves):
-                    x_copy(k, h).wait_recv()
-            parts.append((peer, k))
+        k = serve_order[i]
+        with jax.named_scope("x%d" % i):
+            for h in range(halves):
+                x_copy(k, h).wait_recv()
         with jax.named_scope("experts%d" % i):
-            result = hidden_of(parts)
-            if i:
-                hid_send[k] = result[-cap:]
-                go(hid_copy(k))
-            if i < groups:
-                hid_own[serve_order[i]] = result[:cap]
+            result = hidden_of([(own, k), (peer, k)])
+            hid_send[k] = result[cap:]
+            go(hid_copy(k))
+            hid_own[k] = result[:cap]
 
     sub_c = lax.broadcasted_iota(jnp.int32, (cap, rows), 0)
     lane_c = lax.broadcasted_iota(jnp.int32, (cap, rows), 1)
@@ -519,42 +576,43 @@
         store.start()
         stores.append(store)
 
-    spread_ref[...] = spread.astype(bf)
-    stores = [pltpu.make_async_copy(spread_ref, spread_hbm, outs.at[groups * halves])]
-    stores[0].start()
-    gather_rows(pick, att[tp], am_near[...])
     for h in range(halves):
         near_project(h)
         emit(0, h)
+    from_x[0].wait_recv()
+    go(d_part(0, dv_mate, 2, {"tp": across}))
     for h in range(halves):
-        emit(1, h)
-        relay(0, h)
+        go(y_copy(here, h))
+    emit(1, 0)
+    relay(0, 0)
+    emit(1, 1)
+    relay(0, 1)
+    for h in range(halves):
+        emit(2, h)
+        relay(1, h)
     from_x[1].wait_recv()
     to_mate = [go(d_part(j, dv_mate, 3 + j, {"tp": mate})) for j in range(2)]
     experts(0)
-    for h in range(halves):
-        emit(2, h)
-        relay(1, h)
-    experts(1)
-    for h in range(halves - 1):
-        relay(2, h)
+    relay(2, 0)
+    for h in range(1, halves):
+        relay_when(end, 2, h)
     with jax.named_scope("dmate"):
         d_part(2, dv_mate, 2, {"tp": across}).wait_recv()
         to_mate.append(go(d_part(2, dv_mate, 5, {"tp": mate})))
-    emit(here, 0)
+    experts(1)
     for copy in to_mate:
         copy.wait_recv()
     combine(0)
-    relay(2, halves - 1)
+    late = [relay_when(jnp.logical_not(end), 2, h) for h in range(1, halves)]
+    pending += late
+    emit(here, 0)
+    relay(here, 0)
+    emit(here, 1)
     experts(2)
-    for h in range(1, halves):
-        emit(here, h)
-    for h in range(halves):
-        relay(here, h)
+    relay(here, 1)
     combine(1)
-    experts(3)
     combine(2)
-    experts(4)
+    experts(here)
     combine(here)
     for k in (0, 2, here, 1):
         for h in range(halves):

time: 70.3 us -> 68.6 us (0.976)
  Pallas kernels: 69.3 us -> 67.6 us
    pallas_call x1, Pallas kernels: 66.5 us -> 64.9 us  [mixture(): pl.pallas_call(functools.partial(moe_kernel, groups, HALVES), out_shape=(...]
where the time goes in v4:
time: 68.6 us; the launch traced here: 67.8 us
  Pallas kernels  67.6 us (99%)
    pallas_call x1, Pallas kernels, mixture(): pl.pallas_call(functools.partial(moe_kernel, groups, HALVES), out_shape=(...  64.9 us
    pallas_call x1, Pallas kernels, mixture(): pl.pallas_call(place_kernel, out_shape=jax.ShapeDtypeStruct((rows, width)...  2.74 us

profile of v4, /device:TPU:8, one launch (start us, length us, event | category | flops | bytes accessed | tf_op | source)
XLA Modules:
  0.0 67.8 jit_solution(12650618902305842474)
XLA Ops:
  0.0 64.9 %mixture.1 = (bf16[256,2048]{1,0:T(8,128)(2,1)}, bf16[256,256]{1,0:T(8,128)(2,1)}) custom-call(f32[8]{0:T(128)} %sink_hbm.1, s32[8,128]{1,0:T(8,128)} %bitcast.9, s32[2,256]{1,0:T(2,128)} %bitcast.10, f32[2,256]{1,0:T(2,128)} %bitcast.11, f32[1,2048]{1,0:T(1,128)} %bitcast.8, bf16[1024,512]{1,0:T(8,128)(2,1)} %q_hbm.1, bf16[8,128,128]{2,1,0:T(8,128)(2,1)} %bitcast.6, ...), custom_call_target="tpu_custom_call" | custom-call | tf_op jit(solution)/shard_map/mixture/pallas_call | solution.py:890
  64.9 2.7 %place.1 = bf16[256,2048]{1,0:T(8,128)(2,1)} custom-call(bf16[256,256]{1,0:T(8,128)(2,1)} %get-tuple-element.7.spread_hbm, bf16[256,2048]{1,0:T(8,128)(2,1)} %get-tuple-element.8.rows_hbm), custom_call_target="tpu_custom_call" | custom-call | tf_op jit(solution)/shard_map/place/pallas_call | solution.py:933

commit v5 on v4

--- a/solution.py
+++ b/solution.py
@@ -110,7 +110,7 @@
     qv, resv, wv, w_mate, kx, vx, dl, dr, dx, att, am_far, am_near, routes_far,
     mixed_att, acc, ysend, yrecv, send, own, peer, comb, ret, hid_own, hid_send, hid_recv,
     wsend, wrecv, gv, uv, dv, dv_mate,
-    ls, hs, hr, ms, mr, ys, yr, zs, zr, xs, xr, gs, gr, bs, br, ws, wr, ds, dr_sem, outs,
+    ls, hs, hr, ms, mr, ys, yr, zs, zr, xs, xr, gs, gr, bs, br, ws, wr, ds, dr_sem, outs, known,
 ):
     sp = lax.axis_index("sp")
     tp = lax.axis_index("tp")
@@ -160,10 +160,17 @@
         return {"sp": plane * 2 + side}
 
     barrier = pltpu.get_barrier_semaphore()
-    partners = [{"sp": after}, {"sp": before}, {"tp": mate}, {"tp": across}, x_mate]
-    partners += [to_plane(k) for k in away]
-    for where in partners:
-        pl.semaphore_signal(barrier, inc=1, device_id=where, device_id_type=mesh_id)
+
+    def signal(sem, where):
+        pl.semaphore_signal(sem, inc=1, device_id=where, device_id_type=mesh_id)
+
+    for where in ({"tp": mate}, {"tp": across}, x_mate):
+        signal(barrier, where)
+    pl.when(sp > 0)(lambda: signal(barrier, {"sp": before}))
+    pl.when(sp < sp_count - 1)(lambda: signal(barrier, {"sp": after}))
+    pl.when(gz > 0)(lambda: signal(barrier, {"sp": sp - 2}))
+    pl.when(gz < groups - 1)(lambda: signal(barrier, {"sp": sp + 2}))
+    greeted = 7 - jnp.where((sp == 0) | (sp == sp_count - 1), 1, 0) - jnp.where(end, 1, 0)
     pairs = (
         (k_hbm, kx.at[pl.ds(1, blocks)]), (v_hbm, vx.at[pl.ds(1, blocks)]),
         (doc_hbm, doc_ref), (routes_hbm, routes_ref), (rw_hbm, rw_ref), (sink_hbm, sink_ref),
@@ -187,7 +194,13 @@
     for load in loads[:5]:
         load.wait()
     with jax.named_scope("barrier"):
-        pl.semaphore_wait(barrier, len(partners))
+        pl.semaphore_wait(barrier, greeted)
+
+    @pl.when(jnp.logical_not(end))
+    def _():
+        signal(known, {"sp": sp - 2})
+        signal(known, {"sp": sp + 2})
+
     pending = []
 
     def go(copy):
@@ -260,26 +273,8 @@
         right = jnp.where(sp == sp_count - 1, -1.0, dr[0:1, :].astype(f32))
         dx[blocks + 1] = jnp.broadcast_to(right, (8, WINDOW))
 
-    slot = slots_of(routes_ref[...], order, cap)
     ri = lax.broadcasted_iota(jnp.int32, (rows, rows), 0)
     ci = lax.broadcasted_iota(jnp.int32, (rows, rows), 1)
-    slot_col = jnp.sum(jnp.where(ri == ci, slot, 0.0), axis=1, keepdims=True)
-    spread = jnp.where(slot_col == ci.astype(f32), 1.0, 0.0)
-    weight_rows = []
-    for parity in (side, 1 - side):
-        w_row = jnp.where(routes_ref[0:1, :] % 2 == parity, rw_ref[0:1, :], rw_ref[1:2, :])
-        w_col = jnp.sum(jnp.where(ri == ci, w_row, 0.0), axis=1, keepdims=True)
-        weight_rows.append(jnp.sum(spread * w_col, axis=0, keepdims=True))
-    sub8 = lax.broadcasted_iota(jnp.int32, (8, rows), 0)
-    wsend[...] = jnp.where(
-        sub8 == 0, weight_rows[0], jnp.where(sub8 == 1, weight_rows[1], 0.0)
-    )
-
-    wrecv[here] = wsend[...]
-
-    for k in away:
-        go(remote(wsend, wrecv.at[k], ws.at[k], wr.at[k], to_plane(k)))
-
     qi = lax.broadcasted_iota(jnp.int32, (WINDOW, 3 * WINDOW), 0)
     ki = lax.broadcasted_iota(jnp.int32, (WINDOW, 3 * WINDOW), 1)
     band = (ki >= qi) & (ki <= qi + 2 * WINDOW)
@@ -366,6 +361,11 @@
             for copy in from_x:
                 copy.start()
 
+        @pl.when((i == 1) & jnp.logical_not(end))
+        def _():
+            pl.semaphore_wait(known, 1)
+            signal(known, {"sp": (gz - 1) * (groups - 1) * 2 + side})
+
         @pl.when((i == 2) & jnp.logical_not(early))
         def _():
             near_copy.start()
@@ -444,6 +444,28 @@
         for k in emit_order[1:here]:
             for h in range(halves):
                 go(y_copy(k, h))
+
+    slot = slots_of(routes_ref[...], order, cap)
+    slot_col = jnp.sum(jnp.where(ri == ci, slot, 0.0), axis=1, keepdims=True)
+    spread = jnp.where(slot_col == ci.astype(f32), 1.0, 0.0)
+    weight_rows = []
+    for parity in (side, 1 - side):
+        w_row = jnp.where(routes_ref[0:1, :] % 2 == parity, rw_ref[0:1, :], rw_ref[1:2, :])
+        w_col = jnp.sum(jnp.where(ri == ci, w_row, 0.0), axis=1, keepdims=True)
+        weight_rows.append(jnp.sum(spread * w_col, axis=0, keepdims=True))
+    sub8 = lax.broadcasted_iota(jnp.int32, (8, rows), 0)
+    wsend[...] = jnp.where(
+        sub8 == 0, weight_rows[0], jnp.where(sub8 == 1, weight_rows[1], 0.0)
+    )
+
+    wrecv[here] = wsend[...]
+
+    @pl.when(end)
+    def _():
+        pl.semaphore_wait(known, 2)
+
+    for k in away:
+        go(remote(wsend, wrecv.at[k], ws.at[k], wr.at[k], to_plane(k)))
 
     with jax.named_scope("attn_near"):
         pl.when(tp < 2)(left_halo)
@@ -918,7 +940,7 @@
             per_piece, per_piece, per_piece, per_piece, per_piece, per_piece,
             dma((groups,)), dma((groups,)), per_piece, per_piece,
             dma((groups,)), dma((groups,)), dma((6,)), dma((6,)),
-            dma((groups * HALVES + 1,)),
+            dma((groups * HALVES + 1,)), pltpu.SemaphoreType.REGULAR,
         ],
         compiler_params=pltpu.CompilerParams(
             collective_id=3, has_side_effects=True, vmem_limit_bytes=56 * 1024 * 1024

time: 68.6 us -> 68.6 us (level)
  Pallas kernels: 67.6 us -> 68.3 us
    pallas_call x1, Pallas kernels: 64.9 us -> 65.6 us  [mixture(): pl.pallas_call(functools.partial(moe_kernel, groups, HALVES), out_shape=(...]
where the time goes in v5:
time: 68.6 us; the launch traced here: 68.5 us
  Pallas kernels  68.3 us (100%)
    pallas_call x1, Pallas kernels, mixture(): pl.pallas_call(functools.partial(moe_kernel, groups, HALVES), out_shape=(...  65.6 us
    pallas_call x1, Pallas kernels, mixture(): pl.pallas_call(place_kernel, out_shape=jax.ShapeDtypeStruct((rows, width)...  2.71 us

profile of v5, /device:TPU:8, one launch (start us, length us, event | category | flops | bytes accessed | tf_op | source)
XLA Modules:
  0.0 68.5 jit_solution(4465964085675694250)
XLA Ops:
  0.0 65.6 %mixture.1 = (bf16[256,2048]{1,0:T(8,128)(2,1)}, bf16[256,256]{1,0:T(8,128)(2,1)}) custom-call(f32[8]{0:T(128)} %sink_hbm.1, s32[8,128]{1,0:T(8,128)} %bitcast.9, s32[2,256]{1,0:T(2,128)} %bitcast.10, f32[2,256]{1,0:T(2,128)} %bitcast.11, f32[1,2048]{1,0:T(1,128)} %bitcast.8, bf16[1024,512]{1,0:T(8,128)(2,1)} %q_hbm.1, bf16[8,128,128]{2,1,0:T(8,128)(2,1)} %bitcast.6, ...), custom_call_target="tpu_custom_call" | custom-call | tf_op jit(solution)/shard_map/mixture/pallas_call | solution.py:912
  65.6 2.7 %place.1 = bf16[256,2048]{1,0:T(8,128)(2,1)} custom-call(bf16[256,256]{1,0:T(8,128)(2,1)} %get-tuple-element.7.spread_hbm, bf16[256,2048]{1,0:T(8,128)(2,1)} %get-tuple-element.8.rows_hbm), custom_call_target="tpu_custom_call" | custom-call | tf_op jit(solution)/shard_map/place/pallas_call | solution.py:955

commit v6 on v5

--- a/solution.py
+++ b/solution.py
@@ -356,29 +356,29 @@
         def _():
             send_before()
 
-        @pl.when(i == 1)
+        @pl.when((i == 1) & jnp.logical_not(end))
+        def _():
+            pl.semaphore_wait(known, 1)
+            signal(known, {"sp": (gz - 1) * (groups - 1) * 2 + side})
+
+        @pl.when((i == 2) & jnp.logical_not(early))
+        def _():
+            near_copy.start()
+
+        @pl.when((i == 2) & low_side)
+        def _():
+            with jax.named_scope("halo_right"):
+                right_halo()
+
+        @pl.when((i == 2) & jnp.logical_not(low_side))
+        def _():
+            with jax.named_scope("halo_left"):
+                left_halo()
+
+        @pl.when(i == 2)
         def _():
             for copy in from_x:
                 copy.start()
-
-        @pl.when((i == 1) & jnp.logical_not(end))
-        def _():
-            pl.semaphore_wait(known, 1)
-            signal(known, {"sp": (gz - 1) * (groups - 1) * 2 + side})
-
-        @pl.when((i == 2) & jnp.logical_not(early))
-        def _():
-            near_copy.start()
-
-        @pl.when((i == 2) & low_side)
-        def _():
-            with jax.named_scope("halo_right"):
-                right_halo()
-
-        @pl.when((i == 2) & jnp.logical_not(low_side))
-        def _():
-            with jax.named_scope("halo_left"):
-                left_halo()
 
         attend_home(jnp.where(i == 0, starts[0], jnp.where(i == 1, starts[1], starts[2])))
         return carry
@@ -959,7 +959,7 @@
         out_specs=hbm,
         scratch_shapes=[
             pltpu.VMEM((rows, rows), bf), pltpu.VMEM((rows, width), bf),
-            pltpu.VMEM((rows, width), bf), dma((5,)), dma((4,)),
+            pltpu.VMEM((rows, width), bf), dma((3,)), dma((2,)),
         ],
         name="place",
     )(spread, moved)

time: 68.6 us -> 68 us (level)
  no operation moved by 1% of the time
where the time goes in v6:
time: 68 us; the launch traced here: 67.9 us
  Pallas kernels  67.7 us (100%)
    pallas_call x1, Pallas kernels, mixture(): pl.pallas_call(functools.partial(moe_kernel, groups, HALVES), out_shape=(...  65.1 us
    pallas_call x1, Pallas kernels, mixture(): pl.pallas_call(place_kernel, out_shape=jax.ShapeDtypeStruct((rows, width)...  2.56 us

profile of v6, /device:TPU:8, one launch (start us, length us, event | category | flops | bytes accessed | tf_op | source)
XLA Modules:
  0.0 67.9 jit_solution(15922718503687916114)
XLA Ops:
  0.0 65.1 %mixture.1 = (bf16[256,2048]{1,0:T(8,128)(2,1)}, bf16[256,256]{1,0:T(8,128)(2,1)}) custom-call(f32[8]{0:T(128)} %sink_hbm.1, s32[8,128]{1,0:T(8,128)} %bitcast.9, s32[2,256]{1,0:T(2,128)} %bitcast.10, f32[2,256]{1,0:T(2,128)} %bitcast.11, f32[1,2048]{1,0:T(1,128)} %bitcast.8, bf16[1024,512]{1,0:T(8,128)(2,1)} %q_hbm.1, bf16[8,128,128]{2,1,0:T(8,128)(2,1)} %bitcast.6, ...), custom_call_target="tpu_custom_call" | custom-call | tf_op jit(solution)/shard_map/mixture/pallas_call | solution.py:912
  65.2 2.6 %place.1 = bf16[256,2048]{1,0:T(8,128)(2,1)} custom-call(bf16[256,256]{1,0:T(8,128)(2,1)} %get-tuple-element.7.spread_hbm, bf16[256,2048]{1,0:T(8,128)(2,1)} %get-tuple-element.8.rows_hbm), custom_call_target="tpu_custom_call" | custom-call | tf_op jit(solution)/shard_map/place/pallas_call | solution.py:955
